TPU v7x, 32 devices: a whole 2x2x4 slice. The times are simulated.
32 devices in a mesh: sp: 8 (over z, x), tp: 4 (over y, core).
Axes of the slice: x: 2, y: 2, z: 4, core: 2. Of those that a mesh axis runs over, the one named last changes fastest.
Arguments:
- tokens: bfloat16 [1024, 2048], P('sp', 'tp'), may hold values from -6 to 6
- conv_value_weight: bfloat16 [2048, 1024], P('sp', 'tp'), may hold values from -0.125 to 0.125
- conv_gate_weight: bfloat16 [2048, 1024], P('sp', 'tp'), may hold values from -0.125 to 0.125
- conv_kernel: bfloat16 [31, 1024], P(None, 'tp'), may hold values from -16 to 16
- conv_norm_gain: float32 [1024], P('tp'), may hold values from 0.1 to 1.9
- query_weight: bfloat16 [2048, 2048], P('sp', 'tp'), may hold values from -0.125 to 0.125
- key_weight: bfloat16 [2048, 2048], P('sp', 'tp'), may hold values from -0.125 to 0.125
- value_weight: bfloat16 [2048, 2048], P('sp', 'tp'), may hold values from -0.125 to 0.125
- input_gate_weight: bfloat16 [2048, 8], P(None, 'tp'), may hold values from -0.125 to 0.125
- forget_gate_weight: bfloat16 [2048, 8], P(None, 'tp'), may hold values from -0.125 to 0.125
- input_offset: float32 [1024, 8], P('sp', 'tp'), may hold values from -4 to 210
- forget_offset: float32 [1024, 8], P('sp', 'tp'), may hold values from 0 to 30
- memory_norm_gain: float32 [2048], P('tp'), may hold values from 0.1 to 1.9
- conv_out_weight: bfloat16 [1024, 2048], P('tp', 'sp'), may hold values from -0.3125 to 0.3125
- memory_out_weight: bfloat16 [2048, 2048], P('tp', 'sp'), may hold values from -0.125 to 0.125
Outputs:
- mixed: bfloat16 [1024, 2048], P('sp', 'tp')
All inputs are finite; a program needn't handle non-finite values.
Results may differ from a plain program's by a relative error of at most 0.03.
Values may be sent and summed in bfloat16 or wider, within the bound.
A program may use at most 128 MiB of HBM per device.

v0:
```python
import jax
import jax.numpy as jnp
from jax import lax
from jax.sharding import PartitionSpec as P

BLOCK = 64


EPS = 1e-06
LOWEST_LEVEL = -1e30


def shifted_2(value, axis, steps):
    count = lax.axis_size(axis)
    leading, last = (max(0, -steps), min(count, count - steps))
    return lax.ppermute(value, axis, [(source, source + steps) for source in range(leading, last)])


def carried_in(shard, axis, join, neutral):
    place = lax.axis_index(axis)
    gathered = jax.tree.map(
        lambda a, kind: lax.all_gather(a.astype(kind), axis),
        shard,
        (jnp.bfloat16, jnp.bfloat16, jnp.bfloat16, jnp.bfloat16),
    )
    state = jax.tree.map(lambda a, e: jnp.zeros_like(a) + jnp.asarray(e, a.dtype), shard, neutral)

    def one(step, state):
        return join(
            state,
            jax.tree.map(
                lambda a, own: lax.dynamic_index_in_dim(a, step, 0, False).astype(own.dtype),
                gathered,
                shard,
            ),
        )

    return lax.fori_loop(0, place, one, state)


def block_step(carry, inputs):
    state, normal, level = carry
    query, key, value, gate_in, forget_log = inputs
    length = gate_in.shape[-1]
    scale = query.shape[-1] ** (-0.5)
    causal = jnp.tril(jnp.ones((length, length), dtype=bool))
    within = jnp.cumsum(forget_log, axis=-1)
    log_weight = within[:, :, None] - within[:, None, :] + gate_in[:, None, :]
    log_weight = jnp.where(causal, log_weight, -jnp.inf)
    carried = within + level[:, None]
    top = jnp.maximum(carried, jnp.max(log_weight, axis=-1))
    weight = jnp.exp(log_weight - top[:, :, None])
    carried_weight = jnp.exp(carried - top) * scale
    scores = jnp.einsum("htd,hsd->hts", query, key, preferred_element_type=jnp.float32) * (
        scale * weight
    )
    numer = jnp.einsum(
        "hts,hse->hte", scores.astype(jnp.bfloat16), value, preferred_element_type=jnp.float32
    )
    numer = numer + carried_weight[:, :, None] * jnp.einsum(
        "hed,htd->hte", state.astype(jnp.bfloat16), query, preferred_element_type=jnp.float32
    )
    denom = jnp.sum(scores, axis=-1) + carried_weight * jnp.einsum(
        "hd,htd->ht", normal.astype(jnp.bfloat16), query, preferred_element_type=jnp.float32
    )
    result = numer / jnp.maximum(jnp.abs(denom), 1.0)[:, :, None]
    last = within[:, -1]
    end_log = last[:, None] - within + gate_in
    new_level = jnp.maximum(last + level, jnp.max(end_log, axis=-1))
    keep = jnp.exp(last + level - new_level)
    fresh = jnp.exp(end_log - new_level[:, None])
    scaled_key = (fresh[:, :, None] * key).astype(jnp.bfloat16)
    new_state = keep[:, None, None] * state + jnp.einsum(
        "hse,hsd->hed", value, scaled_key, preferred_element_type=jnp.float32
    )
    new_normal = keep[:, None] * normal + jnp.sum(scaled_key.astype(jnp.float32), axis=1)
    return ((new_state, new_normal, new_level), result)


def depthwise(extended, kernel):
    taps = kernel.shape[0]
    length = extended.shape[0] - taps + 1
    total = extended[0:length] * kernel[0]
    for index in range(1, taps):
        total = total + extended[index : index + length] * kernel[index]
    return total


def merge_states(first, second):
    first_state, first_normal, first_level, first_total = first
    second_state, second_normal, second_level, second_total = second
    shifted = first_level + second_total
    level = jnp.maximum(shifted, second_level)
    older = jnp.exp(shifted - level)
    newer = jnp.exp(second_level - level)
    state = older[:, None, None] * first_state + newer[:, None, None] * second_state
    normal = older[:, None] * first_normal + newer[:, None] * second_normal
    return (state, normal, level, first_total + second_total)


def on_device(
    tokens,
    conv_value_weight,
    conv_gate_weight,
    conv_kernel,
    conv_norm_gain,
    query_weight,
    key_weight,
    value_weight,
    input_gate_weight,
    forget_gate_weight,
    input_offset,
    forget_offset,
    memory_norm_gain,
    conv_out_weight,
    memory_out_weight,
):
    length = tokens.shape[0]
    heads_here = input_gate_weight.shape[1]
    whole = lax.all_gather(tokens, "tp", axis=1, tiled=True)
    pieces = (
        lax.all_gather(conv_value_weight, "sp", axis=0, tiled=True),
        lax.all_gather(conv_gate_weight, "sp", axis=0, tiled=True),
        lax.all_gather(query_weight, "sp", axis=0, tiled=True),
        lax.all_gather(key_weight, "sp", axis=0, tiled=True),
        lax.all_gather(value_weight, "sp", axis=0, tiled=True),
    )
    folded = tuple((jnp.dot(whole, piece, preferred_element_type=jnp.float32) for piece in pieces))
    conv_value, conv_gate, query_flat, key_flat, value_flat = folded
    gate_pre = jnp.dot(whole, input_gate_weight, preferred_element_type=jnp.float32)
    forget_pre = jnp.dot(whole, forget_gate_weight, preferred_element_type=jnp.float32)
    glu = (conv_value * jax.nn.sigmoid(conv_gate)).astype(jnp.bfloat16)
    taps = conv_kernel.shape[0]
    head_dim = query_flat.shape[1] // heads_here

    def to_heads(flat):
        return flat.astype(jnp.bfloat16).reshape(length, heads_here, head_dim).transpose(1, 0, 2)

    query = to_heads(query_flat)
    key = to_heads(key_flat)
    value = to_heads(value_flat)
    gate_in = (gate_pre + input_offset).T
    forget_log = jax.nn.log_sigmoid(forget_pre + forget_offset).T
    within = jnp.cumsum(forget_log, axis=1)
    total = within[:, -1]
    end_log = total[:, None] - within + gate_in
    local_level = jnp.max(end_log, axis=1)
    fresh = jnp.exp(end_log - local_level[:, None])
    scaled_key = (fresh[:, :, None] * key).astype(jnp.bfloat16)
    local_state = jnp.einsum("hse,hsd->hed", value, scaled_key, preferred_element_type=jnp.float32)
    local_normal = jnp.sum(scaled_key.astype(jnp.float32), axis=1)
    blank_state = (
        jnp.zeros_like(local_state),
        jnp.zeros_like(local_normal),
        jnp.full_like(local_level, LOWEST_LEVEL),
        jnp.zeros_like(total),
    )
    prior = shifted_2(glu[length - (taps - 1) :], "sp", 1)
    incoming = carried_in(
        (local_state, local_normal, local_level, total), "sp", merge_states, blank_state
    )
    extended = jnp.concatenate([prior, glu], axis=0).astype(jnp.float32)
    conv = depthwise(extended, conv_kernel.astype(jnp.float32))
    blocks = length // BLOCK

    def split(array):
        return jnp.moveaxis(array.reshape((heads_here, blocks, BLOCK) + array.shape[2:]), 1, 0)

    _, hidden = lax.scan(
        block_step,
        tuple(incoming[:3]),
        (split(query), split(key), split(value), split(gate_in), split(forget_log)),
    )
    hidden = jnp.moveaxis(hidden, 0, 1).reshape(heads_here, length, head_dim)
    hidden_squares = jnp.sum(hidden * hidden, axis=(0, 2))
    channel_sum, channel_squares, memory_squares = lax.psum(
        (jnp.sum(conv, axis=1), jnp.sum(conv * conv, axis=1), hidden_squares), "tp"
    )
    channels = conv.shape[1] * lax.axis_size("tp")
    mean = (channel_sum / channels)[:, None]
    variance = (channel_squares / channels)[:, None] - mean * mean
    conv_branch = jax.nn.silu((conv - mean) * lax.rsqrt(variance + EPS) * conv_norm_gain).astype(
        jnp.bfloat16
    )
    entries = heads_here * head_dim * lax.axis_size("tp")
    memory_scale = lax.rsqrt(memory_squares / entries + EPS)
    hidden = hidden * memory_scale[None, :, None]
    hidden = hidden * memory_norm_gain.reshape(heads_here, 1, head_dim)
    memory_branch = (
        hidden.transpose(1, 0, 2).reshape(length, heads_here * head_dim).astype(jnp.bfloat16)
    )
    conv_columns, memory_columns = (
        lax.all_gather(conv_out_weight, "sp", axis=1, tiled=True),
        lax.all_gather(memory_out_weight, "sp", axis=1, tiled=True),
    )
    contract = (((0,), (1,)), ((), ()))
    summed = lax.psum_scatter(
        (
            lax.dot_general(conv_columns, conv_branch, contract, preferred_element_type=jnp.float32)
            + lax.dot_general(
                memory_columns, memory_branch, contract, preferred_element_type=jnp.float32
            )
        ).astype(jnp.bfloat16),
        "tp",
        scatter_dimension=0,
        tiled=True,
    ).astype(jnp.float32)
    return summed.T.astype(jnp.bfloat16)


def solution(mesh):
    in_specs = (
        P("sp", "tp"),
        P("sp", "tp"),
        P("sp", "tp"),
        P(None, "tp"),
        P("tp"),
        P("sp", "tp"),
        P("sp", "tp"),
        P("sp", "tp"),
        P(None, "tp"),
        P(None, "tp"),
        P("sp", "tp"),
        P("sp", "tp"),
        P("tp"),
        P("tp", "sp"),
        P("tp", "sp"),
    )
    out_specs = P("sp", "tp")
    return jax.shard_map(
        on_device, mesh=mesh, in_specs=in_specs, out_specs=out_specs, check_vma=False
    )
```

profile of v0, /device:TPU:0, one launch (start us, length us, event | category | flops | bytes accessed | tf_op | source)
XLA Modules:
  0.0 414.2 jit_solution(13057960020475259592)
XLA Ops:
  10.0 8.9 %all_gather.44 = bf16[128,2048]{1,0:T(8,128)(2,1)S(1)} all-gather(bf16[128,512]{1,0:T(8,128)(2,1)} %param.19), channel_id=1, replica_groups=mesh['sp'=8,'tp'=4] {'tp'}, dimensions={1}, use_global_device_ids=true | all-gather | bytes 655360 | tf_op jit(solution)/shard_map/all_gather | solution.py:120
  18.8 1.0 fusion.87
  20.8 41.0 %all-gather.22.cloned.1.call-done = bf16[2048,512]{1,0:T(8,128)(2,1)} async-done(((bf16[256,512]{1,0:T(8,128)(2,1)}), bf16[2048,512]{1,0:T(8,128)(2,1)}) %all-gather.22.cloned.1.call-update) | async-done | bytes 2097168 | tf_op jit(solution)/shard_map/all_gather | solution.py:125
  61.7 2.0 convolution_convert_fusion.2
  63.8 47.7 %all-gather.20.cloned.1.call-done = bf16[2048,512]{1,0:T(8,128)(2,1)} async-done(((bf16[256,512]{1,0:T(8,128)(2,1)}), bf16[2048,512]{1,0:T(8,128)(2,1)}) %all-gather.20.cloned.1.call-update) | async-done | bytes 2097168 | tf_op jit(solution)/shard_map/all_gather | solution.py:126
  111.5 2.0 convolution_convert_fusion.3
  113.5 1.0 convolution_convert_fusion
  118.1 34.3 %all-gather.14.cloned.1.call-done = bf16[2048,256]{1,0:T(8,128)(2,1)} async-done(((bf16[256,256]{1,0:T(8,128)(2,1)}), bf16[2048,256]{1,0:T(8,128)(2,1)}) %all-gather.14.cloned.1.call-update) | async-done | bytes 1048592 | tf_op jit(solution)/shard_map/all_gather | solution.py:122
  152.5 1.5 fusion.99
  154.0 39.5 %all-gather.16.cloned.1.call-done = bf16[2048,256]{1,0:T(8,128)(2,1)} async-done(((bf16[256,256]{1,0:T(8,128)(2,1)}), bf16[2048,256]{1,0:T(8,128)(2,1)}) %all-gather.16.cloned.1.call-update) | async-done | bytes 1048592 | tf_op jit(solution)/shard_map/all_gather | solution.py:123
  193.5 1.6 fusion.43
  195.1 2.5 collective-permute-start
  197.6 18.5 %all-reduce.3 = (bf16[16]{0:T(256)(128)(2,1)S(1)}, bf16[16]{0:T(256)(128)(2,1)S(1)}) all-reduce(bf16[16]{0:T(256)(128)(2,1)S(1)} %dynamic-update-slice, bf16[16]{0:T(256)(128)(2,1)S(1)} %dynamic-update-slice.1), channel_id=2, replica_groups=mesh['sp'=8,'tp'=4] {'sp'}, use_global_device_ids=true, to_apply=%add | all-reduce | flops 32 | bytes 128
  217.2 17.5 %all-gather.4 = bf16[8,2,256]{2,1,0:T(2,128)(2,1)S(1)} all-gather(bf16[1,2,256]{2,1,0:T(2,128)(2,1)S(1)} %bitcast.242), channel_id=5, replica_groups=mesh['sp'=8,'tp'=4] {'sp'}, dimensions={0}, use_global_device_ids=true | all-gather | bytes 9216 | tf_op jit(solution)/shard_map/all_gather | solution.py:22
  234.7 8.8 %all-gather.24.cloned.1.call-done = bf16[2048,512]{1,0:T(8,128)(2,1)} async-done(((bf16[256,512]{1,0:T(8,128)(2,1)}), bf16[2048,512]{1,0:T(8,128)(2,1)}) %all-gather.24.cloned.1.call-update) | async-done | bytes 2097168 | tf_op jit(solution)/shard_map/all_gather | solution.py:124
  243.5 2.0 convolution_convert_fusion.1
  245.6 47.6 %all-gather.28.cloned.1.call-done = bf16[16,256,256]{2,1,0:T(8,128)(2,1)} async-done(((bf16[2,256,256]{2,1,0:T(8,128)(2,1)}), bf16[16,256,256]{2,1,0:T(8,128)(2,1)}) %all-gather.28.cloned.1.call-update) | async-done | bytes 2097168 | tf_op jit(solution)/shard_map/all_gather | solution.py:22
  293.3 4.7 %while.33 = (s32[]{:T(128)}, f32[2,256,256]{2,1,0:T(8,128)S(1)}, f32[2,256]{1,0:T(2,128)S(1)}, f32[2]{0:T(128)S(1)}, f32[2,2,64,256]{3,2,0,1:T(8,128)S(1)}, /*in...) while((s32[]{:T(128)}, f32[2,256,256]{2,1,0:T(8,128)S(1)}, ...), condition=%wide.region_15.16_spmd, body=%wide.region_9.15_spmd.sunk | while | flops 42875268 | bytes 2589957 | solution.py:169
  298.2 5.6 %all-reduce.2 = (f32[128]{0:T(128)S(1)}, f32[128]{0:T(128)S(1)}, f32[128]{0:T(128)S(1)}) all-reduce(f32[128]{0:T(128)S(1)} %get-tuple-element.156, f32[128]{0:T(128)S(1)} %get-tuple-element.155, f32[128]{0:T(128)S(1)} %reduce_sum.63), channel_id=1, replica_groups=mesh['sp'=8,'tp'=4] {'tp'}, use_global_device_ids=true, to_apply=%region_3.4 | all-reduce | flops 384 | bytes 3072 | tf_op jit(solution)/shard_map/psum | solution.py:176
  304.1 29.3 %all-gather.18.cloned.1.call-done = bf16[256,2048]{1,0:T(8,128)(2,1)} async-done(((bf16[256,256]{1,0:T(8,128)(2,1)}), bf16[256,2048]{1,0:T(8,128)(2,1)}) %all-gather.18.cloned.1.call-update) | async-done | bytes 1048592 | tf_op jit(solution)/shard_map/all_gather | solution.py:193
  333.4 1.6 fusion.81
  335.0 49.8 %all-gather.26.cloned.1.call-done = bf16[512,2048]{1,0:T(8,128)(2,1)} async-done(((bf16[512,256]{1,0:T(8,128)(2,1)}), bf16[512,2048]{1,0:T(8,128)(2,1)}) %all-gather.26.cloned.1.call-update) | async-done | bytes 2097168 | tf_op jit(solution)/shard_map/all_gather | solution.py:194
  384.8 2.9 fusion.38
  387.7 20.0 %reduce-scatter.2.cloned.1.call-done = bf16[512,128]{0,1:T(8,128)(2,1)} async-done(((bf16[2048,128]{0,1:T(8,128)(2,1)}), bf16[512,128]{0,1:T(8,128)(2,1)}) %reduce-scatter.2.cloned.1.call-update) | async-done | bytes 131088 | tf_op jit(solution)/shard_map/reduce_scatter | solution.py:197
  (105 shorter events, 13.3 us)
Async XLA Ops:
  6.5 13.8 %copy-start = (bf16[2048,2]{0,1:T(2,128)(2,1)S(1)}, bf16[2048,2]{0,1:T(2,128)(2,1)}, u32[]{:S(2)}) copy-start(bf16[2048,2]{0,1:T(2,128)(2,1)} %param.27) | copy-start | bytes 24580
  6.5 13.8 %copy-start.4 = (f32[128,2]{0,1:T(2,128)S(1)}, f32[128,2]{0,1:T(2,128)}, u32[]{:S(2)}) copy-start(f32[128,2]{0,1:T(2,128)} %param.29) | copy-start | bytes 3076
  6.5 55.2 %all-gather.22.cloned.1.call-start = ((), (), s32[]{:S(2)}) async-start(), calls=%async_computation.5 | async-start | bytes 2359296 | tf_op jit(solution)/shard_map/all_gather | solution.py:125
  7.3 104.2 %all-gather.20.cloned.1.call-start = ((), (), s32[]{:S(2)}) async-start(), calls=%async_computation.4 | async-start | bytes 2359296 | tf_op jit(solution)/shard_map/all_gather | solution.py:126
  8.0 144.5 %all-gather.14.cloned.1.call-start = ((), (), s32[]{:S(2)}) async-start(), calls=%async_computation.1 | async-start | bytes 1179648 | tf_op jit(solution)/shard_map/all_gather | solution.py:122
  8.7 184.7 %all-gather.16.cloned.1.call-start = ((), (), s32[]{:S(2)}) async-start(), calls=%async_computation.2 | async-start | bytes 1179648 | tf_op jit(solution)/shard_map/all_gather | solution.py:123
  9.3 234.2 %all-gather.24.cloned.1.call-start = ((), (), s32[]{:S(2)}) async-start(), calls=%async_computation.6 | async-start | bytes 2359296 | tf_op jit(solution)/shard_map/all_gather | solution.py:124
  9.9 283.3 %all-gather.28.cloned.1.call-start = ((), (), s32[]{:S(2)}) async-start(), calls=%async_computation.9 | async-start | bytes 2359296 | tf_op jit(solution)/shard_map/all_gather | solution.py:22
  63.8 52.6 %copy-start.1 = (bf16[31,256]{1,0:T(8,128)(2,1)S(1)}, bf16[31,256]{1,0:T(8,128)(2,1)}, u32[]{:S(2)}) copy-start(bf16[31,256]{1,0:T(8,128)(2,1)} %param.22) | copy-start | bytes 47620
  63.8 52.6 %copy-start.5 = (u32[32]{0:T(128)S(1)}, u32[32]{0:T(128)}, u32[]{:S(2)}) copy-start(u32[32]{0:T(128)} %constant.96) | copy-start | bytes 388
  114.6 101.8 %copy-start.2 = (f32[512]{0:T(512)S(1)}, f32[512]{0:T(512)}, u32[]{:S(2)}) copy-start(f32[512]{0:T(512)} %param.31) | copy-start | bytes 6148
  114.6 218.8 %all-gather.18.cloned.1.call-start = ((), (), s32[]{:S(2)}) async-start(), calls=%async_computation.3 | async-start | bytes 1179648 | tf_op jit(solution)/shard_map/all_gather | solution.py:193
  115.4 269.5 %all-gather.26.cloned.1.call-start = ((), (), s32[]{:S(2)}) async-start(), calls=%async_computation.7 | async-start | bytes 2359296 | tf_op jit(solution)/shard_map/all_gather | solution.py:194
  116.1 291.6 %reduce-scatter.2.cloned.1.call-start = ((), (), s32[]{:S(2)}) async-start(), calls=%async_computation.8 | async-start | bytes 655360 | tf_op jit(solution)/shard_map/reduce_scatter | solution.py:197
  195.1 21.4 %collective-permute-start = (bf16[30,256]{1,0:T(8,128)(2,1)S(1)}, bf16[30,256]{1,0:T(8,128)(2,1)S(1)}, u32[]{:S(2)}, u32[]{:S(2)}) collective-permute-start(bf16[30,256]{1,0:T(8,128)(2,1)S(1)} %slice.259), channel_id=1, source_target_pairs={{0,4},{4,8},{8,12},{12,16},{16,20},{20,24},{24,28},{1,5},{5,9},{9,... | collective-permute-start | bytes 46088 | tf_op jit(solution)/shard_map/ppermute | solution.py:16
  293.3 40.1 %copy-start.3 = (f32[256]{0:T(256)S(1)}, f32[256]{0:T(256)}, u32[]{:S(2)}) copy-start(f32[256]{0:T(256)} %param.23) | copy-start | bytes 3076
Sparse Core Ops, SparseCore 0:
  9.5 52.2 all-gather.21
  63.8 47.6 all-gather.19
  113.6 38.7 all-gather.13
  154.5 38.9 all-gather.15
  195.4 48.0 all-gather.23
  245.5 47.6 all-gather.27
  295.2 38.1 all-gather.17
  335.4 49.3 all-gather.25
  387.8 19.8 reduce-scatter.1
where the time goes:
time: 415 us; the launch traced here: 414 us
  waiting for transfers between devices  323 us (78%)
  blocking collectives  50.5 us (12%)
  matrix products  18.2 us (4%)
  between operations  14.1 us (3%)
    all_gather x1, waiting for transfers between devices, on_device(): lax.all_gather(memory_out_weight, 'sp', axis=1, tiled=True)  49.8 us
    all_gather x1, waiting for transfers between devices, on_device(): lax.all_gather(value_weight, 'sp', axis=0, tiled=True)  47.7 us
    all_gather x1, waiting for transfers between devices, carried_in(): lax.all_gather(a.astype(kind), axis)  47.6 us
    all_gather x1, waiting for transfers between devices, on_device(): lax.all_gather(key_weight, 'sp', axis=0, tiled=True)  41 us
    all_gather x1, waiting for transfers between devices, on_device(): lax.all_gather(conv_gate_weight, 'sp', axis=0, tiled=True)  39.5 us
    all_gather x1, waiting for transfers between devices, on_device(): lax.all_gather(conv_value_weight, 'sp', axis=0, tiled=True)  34.3 us
    all_gather x1, waiting for transfers between devices, on_device(): lax.all_gather(conv_out_weight, 'sp', axis=1, tiled=True)  29.3 us
    reduce_scatter x1, waiting for transfers between devices, on_device(): lax.psum_scatter((lax.dot_general(conv_columns, conv_branch, contract, pr...  20 us
  transfers between devices with their start and end apart: 10, of which 9 were waited for; matrix products, arithmetic and copies ran while one was open for 5% of the time, Pallas kernels for 0%

commit v1 on v0

--- a/solution.py
+++ b/solution.py
@@ -98,7 +98,7 @@
     return (state, normal, level, first_total + second_total)
 
 
-def on_device(
+def on_device_by_position(
     tokens,
     conv_value_weight,
     conv_gate_weight,
@@ -208,6 +208,164 @@
     return summed.T.astype(jnp.bfloat16)
 
 
+def forget_parts(forget_log):
+    coarse = jnp.round(forget_log * 8.0) * 0.125
+    return jnp.cumsum(coarse, axis=-1), jnp.cumsum(forget_log - coarse, axis=-1)
+
+
+def exchange_weights(pieces):
+    return lax.all_to_all(pieces, "sp", 0, 0, tiled=False)
+
+
+def gather_tokens(tokens):
+    whole = lax.all_gather(tokens, "tp", axis=1, tiled=True)
+    return lax.all_gather(whole, "sp", axis=0, tiled=True)
+
+
+def gather_in_group(mine, size):
+    count = lax.axis_size("sp")
+    groups = [list(range(first, first + size)) for first in range(0, count, size)]
+    return lax.all_gather(mine, "sp", axis_index_groups=groups)
+
+
+def on_device_by_column(
+    tokens,
+    conv_value_weight,
+    conv_gate_weight,
+    conv_kernel,
+    conv_norm_gain,
+    query_weight,
+    key_weight,
+    value_weight,
+    input_gate_weight,
+    forget_gate_weight,
+    input_offset,
+    forget_offset,
+    memory_norm_gain,
+    conv_out_weight,
+    memory_out_weight,
+):
+    f32, bf16 = jnp.float32, jnp.bfloat16
+    count = lax.axis_size("sp")
+    columns = lax.axis_size("tp")
+    place = lax.axis_index("sp")
+    heads_here = input_gate_weight.shape[1]
+    size = count // heads_here
+    head, quarter = place // size, place % size
+    depth = query_weight.shape[0]
+    head_dim = query_weight.shape[1] // heads_here
+    slab = head_dim // size
+    channels = conv_value_weight.shape[1] // count
+    pieces = jnp.concatenate(
+        [
+            w.reshape(depth, count, -1)
+            for w in (query_weight, key_weight, value_weight, conv_value_weight, conv_gate_weight)
+        ],
+        axis=2,
+    ).transpose(1, 0, 2)
+    weights = exchange_weights(pieces).reshape(count * depth, -1)
+    whole = gather_tokens(tokens)
+    length = whole.shape[0]
+    offsets = lax.all_gather(
+        jnp.concatenate([input_offset, forget_offset], axis=1), "sp", axis=0, tiled=True
+    )
+    gate_weights = jnp.concatenate([input_gate_weight, forget_gate_weight], axis=1)
+    flat = jnp.dot(whole, weights, preferred_element_type=f32)
+    gates = (jnp.dot(whole, gate_weights, preferred_element_type=f32) + offsets).T
+    glu = (
+        flat[:, 3 * slab : 3 * slab + channels] * jax.nn.sigmoid(flat[:, 3 * slab + channels :])
+    ).astype(bf16)
+    parts = gather_in_group(flat[:, : 3 * slab].astype(bf16), size)
+
+    taps = conv_kernel.shape[0]
+    kernel = lax.dynamic_slice_in_dim(conv_kernel, place * channels, channels, 1).astype(f32)
+    extended = jnp.concatenate([jnp.zeros((taps - 1, channels), f32), glu.astype(f32)], axis=0)
+    conv = depthwise(extended, kernel)
+
+    rows = length // size
+    start = quarter * rows
+    gate_in = lax.dynamic_index_in_dim(gates[:heads_here], head, 0, False)
+    forget_log = jax.nn.log_sigmoid(
+        lax.dynamic_index_in_dim(gates[heads_here:], head, 0, False)
+    )
+    coarse, fine = forget_parts(forget_log)
+    mine_coarse = lax.dynamic_slice_in_dim(coarse, start, rows)
+    mine_fine = lax.dynamic_slice_in_dim(fine, start, rows)
+    log_weight = (
+        (mine_coarse[:, None] - coarse[None, :])
+        + (mine_fine[:, None] - fine[None, :])
+        + gate_in[None, :]
+    )
+    causal = (start + jnp.arange(rows))[:, None] >= jnp.arange(length)[None, :]
+    log_weight = jnp.where(causal, log_weight, -jnp.inf)
+    weight = jnp.exp(log_weight - jnp.max(log_weight, axis=1, keepdims=True))
+    query = lax.dynamic_slice_in_dim(parts[:, :, :slab], start, rows, 1)
+    query = query.transpose(1, 0, 2).reshape(rows, head_dim)
+    key = parts[:, :, slab : 2 * slab].transpose(1, 0, 2).reshape(length, head_dim)
+    value = parts[:, :, 2 * slab :].transpose(1, 0, 2).reshape(length, head_dim)
+    scores = jnp.einsum("td,sd->ts", query, key, preferred_element_type=f32) * (
+        weight * head_dim ** (-0.5)
+    )
+    numer = jnp.dot(scores.astype(bf16), value, preferred_element_type=f32)
+    denom = jnp.sum(scores, axis=1)
+    cell = numer / jnp.maximum(jnp.abs(denom), 1.0)[:, None]
+
+    squares = lax.dynamic_update_slice_in_dim(
+        jnp.zeros((length,), f32), jnp.sum(cell * cell, axis=1), start, 0
+    )
+    sums = lax.psum(
+        jnp.stack([jnp.sum(conv, axis=1), jnp.sum(conv * conv, axis=1), squares]), ("sp", "tp")
+    )
+    total = channels * count * columns
+    mean = sums[0] / total
+    variance = sums[1] / total - mean * mean
+    gain = lax.dynamic_slice_in_dim(conv_norm_gain, place * channels, channels)
+    conv_branch = jax.nn.silu(
+        (conv - mean[:, None]) * lax.rsqrt(variance + EPS)[:, None] * gain
+    ).astype(bf16)
+    entries = heads_here * head_dim * columns
+    memory_scale = lax.rsqrt(lax.dynamic_slice_in_dim(sums[2], start, rows) / entries + EPS)
+    memory_gain = lax.dynamic_slice_in_dim(memory_norm_gain, head * head_dim, head_dim)
+    memory_branch = (cell * memory_scale[:, None] * memory_gain).astype(bf16)
+
+    conv_all = lax.all_gather(conv_branch, "sp")
+    memory_all = lax.all_gather(memory_branch, "sp")
+    conv_all = conv_all.transpose(1, 0, 2).reshape(length, -1)
+    memory_all = (
+        memory_all.reshape(heads_here, length, head_dim).transpose(1, 0, 2).reshape(length, -1)
+    )
+    partial = (
+        jnp.dot(conv_all, conv_out_weight, preferred_element_type=f32)
+        + jnp.dot(memory_all, memory_out_weight, preferred_element_type=f32)
+    ).astype(bf16)
+    return send_partials(partial)
+
+
+def send_partials(partial):
+    count, columns = lax.axis_size("sp"), lax.axis_size("tp")
+    length, width = partial.shape
+    swapped = lax.all_to_all(partial.reshape(count, length // count, width), "sp", 0, 0)
+    swapped = swapped.reshape(columns, count // columns, length // count, width)
+    groups = lax.all_to_all(swapped, "tp", 0, 0)
+    summed = jnp.sum(groups.astype(jnp.float32), axis=0).astype(jnp.bfloat16)
+    return summed.transpose(1, 0, 2).reshape(length // count, -1)
+
+
+def splits_by_column(mesh, tokens, query_weight, conv_value_weight, input_gate_weight):
+    count, columns = mesh.shape["sp"], mesh.shape["tp"]
+    heads_here = input_gate_weight.shape[1] // columns
+    head_dim = query_weight.shape[1] // input_gate_weight.shape[1]
+    if count % heads_here or count % columns:
+        return False
+    size = count // heads_here
+    return (
+        tokens.size * 2 <= 8 * 2**20
+        and head_dim % size == 0
+        and tokens.shape[0] % (size * 8) == 0
+        and conv_value_weight.shape[1] % (count * columns) == 0
+    )
+
+
 def solution(mesh):
     in_specs = (
         P("sp", "tp"),
@@ -227,6 +385,12 @@
         P("tp", "sp"),
     )
     out_specs = P("sp", "tp")
-    return jax.shard_map(
-        on_device, mesh=mesh, in_specs=in_specs, out_specs=out_specs, check_vma=False
-    )
+
+    def run(*arrays):
+        by_column = splits_by_column(mesh, arrays[0], arrays[5], arrays[1], arrays[8])
+        on_device = on_device_by_column if by_column else on_device_by_position
+        return jax.shard_map(
+            on_device, mesh=mesh, in_specs=in_specs, out_specs=out_specs, check_vma=False
+        )(*arrays)
+
+    return run

time: 415 us -> 271 us (0.65)
  waiting for transfers between devices: 323 us -> 83.9 us
  blocking collectives: 50.5 us -> 138 us
  local copies, waits for them, and re-layouts: 2.52 us -> 16.7 us
  matrix products: 18.2 us -> 8.81 us
    all_gather x8 -> x3, waiting for transfers between devices: 298 us -> 46.8 us  [the longest x1 37.1 us: gather_tokens(): return lax.all_gather(whole, 'sp', axis=0, tiled=True)]
    all_gather x2 -> x3, blocking collectives: 26.4 us -> 69.6 us  [the longest x1 31.8 us: on_device_by_column(): conv_all = lax.all_gather(conv_branch, 'sp')]
    all_to_all x0 -> x1, waiting for transfers between devices: none -> 37.1 us  [exchange_weights(): return lax.all_to_all(pieces, 'sp', 0, 0, tiled=False)]
    psum x1, blocking collectives: 5.64 us -> 39.6 us  [on_device_by_column(): lax.psum(jnp.stack([jnp.sum(conv, axis=1), jnp.sum(conv * conv, axis=1),...]
    all_to_all x0 -> x2, blocking collectives: none -> 28.5 us  [the longest x1 17.2 us: send_partials(): lax.all_to_all(partial.reshape(count, length // count, width), 'sp', 0, 0)]
    reduce_scatter x1 -> x0, waiting for transfers between devices: 20 us -> none  [on_device(): lax.psum_scatter((lax.dot_general(conv_columns, conv_branch, contract, pr...]
    unnamed x1 -> x0, blocking collectives: 18.5 us -> none
    dot_general x20 -> x6, matrix products: 18.2 us -> 8.81 us  [the longest x1 3.52 us: on_device_by_column(): flat = jnp.dot(whole, weights, preferred_element_type=f32)]
  transfers between devices with their start and end apart: 10 -> 4, of which waited for: 9 -> 4; matrix products, arithmetic and copies ran while one was open for 5% -> 6% of each run, Pallas kernels for 0% -> 0%
where the time goes in v1:
time: 271 us; the launch traced here: 270 us
  blocking collectives  138 us (51%)
  waiting for transfers between devices  83.9 us (31%)
  local copies, waits for them, and re-layouts  16.7 us (6%)
  between operations  13.5 us (5%)
  matrix products  8.81 us (3%)
  starting transfers between devices  5.92 us (2%)
  other arithmetic  3.6 us (1%)
    psum x1, blocking collectives, on_device_by_column(): lax.psum(jnp.stack([jnp.sum(conv, axis=1), jnp.sum(conv * conv, axis=1),...  39.6 us
    all_to_all x1, waiting for transfers between devices, exchange_weights(): return lax.all_to_all(pieces, 'sp', 0, 0, tiled=False)  37.1 us
    all_gather x1, waiting for transfers between devices, gather_tokens(): return lax.all_gather(whole, 'sp', axis=0, tiled=True)  37.1 us
    all_gather x1, blocking collectives, on_device_by_column(): conv_all = lax.all_gather(conv_branch, 'sp')  31.8 us
    all_gather x1, blocking collectives, on_device_by_column(): lax.all_gather(jnp.concatenate([input_offset, forget_offset], axis=1), 's...  27.4 us
    all_to_all x1, blocking collectives, send_partials(): lax.all_to_all(partial.reshape(count, length // count, width), 'sp', 0, 0)  17.2 us
    all_to_all x1, blocking collectives, send_partials(): groups = lax.all_to_all(swapped, 'tp', 0, 0)  11.3 us
    all_gather x1, blocking collectives, gather_tokens(): whole = lax.all_gather(tokens, 'tp', axis=1, tiled=True)  10.4 us
  transfers between devices with their start and end apart: 4, of which 4 were waited for; matrix products, arithmetic and copies ran while one was open for 6% of the time, Pallas kernels for 0%

profile of v1, /device:TPU:0, one launch (start us, length us, event | category | flops | bytes accessed | tf_op | source)
XLA Modules:
  0.0 270.2 jit_solution(7886336359932702150)
XLA Ops:
  6.6 10.4 %all_gather.27 = bf16[128,2048]{1,0:T(8,128)(2,1)} all-gather(bf16[128,512]{1,0:T(8,128)(2,1)} %param.15), channel_id=1, replica_groups=mesh['sp'=8,'tp'=4] {'tp'}, dimensions={1}, use_global_device_ids=true | all-gather | bytes 655360 | tf_op jit(solution)/shard_map/all_gather | solution.py:221
  17.0 1.1 copy.40
  18.1 1.1 copy.41
  19.2 1.1 copy.42
  20.3 1.0 copy.43
  21.3 1.0 copy.44
  25.8 5.8 %all-to-all-start = ((bf16[8,256,256]{1,2,0:T(8,128)(2,1)}), bf16[8,256,256]{1,2,0:T(8,128)(2,1)S(1)}, u32[]{:S(2)}, u32[]{:S(2)}) async-start(bf16[8,256,256]{1,2,0:T(8,128)(2,1)} %bitcast.5), calls=%async_computation | async-start | bytes 2097152 | tf_op jit(solution)/shard_map/all_to_all | solution.py:217
  31.8 37.1 %all-to-all-done = bf16[8,256,256]{1,2,0:T(8,128)(2,1)S(1)} async-done(((bf16[8,256,256]{1,2,0:T(8,128)(2,1)}), bf16[8,256,256]{1,2,0:T(8,128)(2,1)S(1)}, u32[]{:S(2)}, u32[]{:S(2)}) %all-to-all-start) | async-done | bytes 1048608 | tf_op jit(solution)/shard_map/all_to_all | solution.py:217
  69.4 37.1 %all-gather.7.cloned.1.call-done = bf16[1024,2048]{1,0:T(8,128)(2,1)} async-done(((bf16[128,2048]{1,0:T(8,128)(2,1)}), bf16[1024,2048]{1,0:T(8,128)(2,1)}) %all-gather.7.cloned.1.call-update) | async-done | bytes 4194320 | tf_op jit(solution)/shard_map/all_gather | solution.py:222
  106.5 3.5 %convolution_bitcast_fusion.1 = f32[1024,256]{0,1:T(8,128)S(1)} fusion(bf16[2048,256]{1,0:T(8,128)(2,1)S(1)} %bitcast.143, bf16[1024,2048]{1,0:T(8,128)(2,1)} %all-gather.7.cloned.1.call-done), kind=kOutput, calls=%fused_computation.3 | convolution fusion | flops 1073741824 | bytes 6291456 | tf_op jit(solution)/shard_map/dot_general | solution.py:273
  110.0 0.8 slice.659
  111.0 27.4 %all_gather.31 = f32[1024,4]{0,1:T(4,128)S(1)} all-gather(f32[128,4]{0,1:T(4,128)S(1)} %pad_maximum_fusion.1), channel_id=1, replica_groups=mesh['sp'=8,'tp'=4] {'sp'}, dimensions={0}, use_global_device_ids=true | all-gather | bytes 18432 | tf_op jit(solution)/shard_map/all_gather | solution.py:269
  138.5 3.4 %fusion.3 = f32[4,1024]{1,0:T(4,128)S(1)} fusion(f32[1024,4]{0,1:T(4,128)S(1)} %all_gather.31, bf16[1024,2048]{1,0:T(8,128)(2,1)} %all-gather.7.cloned.1.call-done, bf16[2048,2]{0,1:T(2,128)(2,1)S(1)} %copy-done.2, bf16[2048,2]{0,1:T(2,128)(2,1)S(1)} %copy-done.3), kind=kOutput, calls=%fused_computation.8 | convolution fusion | flops 16814080 | bytes 4243456 | tf_op jit(solution)/shard_map/dot_general | solution.py:274
  143.6 1.3 fusion.81
  145.3 2.9 %reshape.162 = bf16[4,1024,192]{1,0,2:T(4,128)(2,1)S(1)} reshape(bf16[4096,192]{0,1:T(8,128)(2,1)} %all-gather.9.cloned.1.call-done) | data formatting | bytes 3145728 | tf_op jit(solution)/shard_map/all_gather | solution.py:228
  148.8 0.7 fusion.85
  150.1 39.6 %psum.7 = f32[3,1024]{1,0:T(4,128)S(1)} all-reduce(f32[3,1024]{1,0:T(4,128)S(1)} %pad_maximum_fusion), channel_id=1, replica_groups=mesh['sp'=8,'tp'=4] {'sp','tp'}, use_global_device_ids=true, to_apply=%region_9.10 | all-reduce | flops 3072 | bytes 24576 | tf_op jit(solution)/shard_map/psum | solution.py:316
  189.8 0.8 multiply_convert_fusion
  190.8 31.8 %all-gather.1 = bf16[8192,32]{0,1:T(8,128)(2,1)S(1)} all-gather(bf16[1024,32]{0,1:T(8,128)(2,1)S(1)} %multiply_convert_fusion.1), channel_id=3, replica_groups=mesh['sp'=8,'tp'=4] {'sp'}, dimensions={0}, use_global_device_ids=true | all-gather | bytes 589824 | tf_op jit(solution)/shard_map/all_gather | solution.py:331
  222.6 9.4 %all-gather.11.cloned.1.call-done = bf16[2048,256]{0,1:T(8,128)(2,1)} async-done(((bf16[256,256]{0,1:T(8,128)(2,1)}), bf16[2048,256]{0,1:T(8,128)(2,1)}) %all-gather.11.cloned.1.call-update) | async-done | bytes 1048592 | tf_op jit(solution)/shard_map/all_gather | solution.py:332
  232.0 1.3 copy.69
  234.2 17.2 %all_to_all.15 = bf16[8,128,256]{2,1,0:T(8,128)(2,1)S(1)} all-to-all(bf16[8,128,256]{2,1,0:T(8,128)(2,1)S(1)} %bitcast.139), channel_id=1, replica_groups=mesh['sp'=8,'tp'=4] {'sp'}, dimensions={0} | all-to-all | bytes 1048576 | tf_op jit(solution)/shard_map/all_to_all | solution.py:347
  251.3 11.3 %all_to_all.16 = bf16[4,2,128,256]{3,2,1,0:T(8,128)(2,1)S(1)} all-to-all(bf16[4,2,128,256]{3,2,1,0:T(8,128)(2,1)S(1)} %bitcast.141), channel_id=1, replica_groups=mesh['sp'=8,'tp'=4] {'tp'}, dimensions={0} | all-to-all | bytes 1048576 | tf_op jit(solution)/shard_map/all_to_all | solution.py:349
  262.9 0.8 copy.52
  (72 shorter events, 9.0 us)
Async XLA Ops:
  6.5 226.8 %copy-start = (bf16[512,256]{1,0:T(8,128)(2,1)S(1)}, bf16[512,256]{1,0:T(8,128)(2,1)}, u32[]{:S(2)}) copy-start(bf16[512,256]{1,0:T(8,128)(2,1)} %param.29) | copy-start | bytes 786436
  6.5 25.1 %copy-start.5 = (f32[128,2]{0,1:T(2,128)S(1)}, f32[128,2]{0,1:T(2,128)}, u32[]{:S(2)}) copy-start(f32[128,2]{0,1:T(2,128)} %param.26) | copy-start | bytes 3076
  6.5 25.1 %copy-start.6 = (f32[128,2]{0,1:T(2,128)S(1)}, f32[128,2]{0,1:T(2,128)}, u32[]{:S(2)}) copy-start(f32[128,2]{0,1:T(2,128)} %param.25) | copy-start | bytes 3076
  6.5 25.1 %copy-start.4 = (bf16[31,256]{1,0:T(8,128)(2,1)S(1)}, bf16[31,256]{1,0:T(8,128)(2,1)}, u32[]{:S(2)}) copy-start(bf16[31,256]{1,0:T(8,128)(2,1)} %param.18) | copy-start | bytes 47620
  6.5 99.9 %all-gather.7.cloned.1.call-start = ((), (), s32[]{:S(2)}) async-start(), calls=%async_computation.3 | async-start | bytes 4718592 | tf_op jit(solution)/shard_map/all_gather | solution.py:222
  25.8 43.1 %all-to-all-start = ((bf16[8,256,256]{1,2,0:T(8,128)(2,1)}), bf16[8,256,256]{1,2,0:T(8,128)(2,1)S(1)}, u32[]{:S(2)}, u32[]{:S(2)}) async-start(bf16[8,256,256]{1,2,0:T(8,128)(2,1)} %bitcast.5), calls=%async_computation | async-start | bytes 2097152 | tf_op jit(solution)/shard_map/all_to_all | solution.py:217
  31.6 113.7 %all-gather.9.cloned.1.call-start = ((), (), s32[]{:S(2)}) async-start(), calls=%async_computation.4 | async-start | bytes 1966080 | tf_op jit(solution)/shard_map/all_gather | solution.py:228
  106.5 4.5 %copy-start.7 = (f32[512]{0:T(512)S(1)}, f32[512]{0:T(512)}, u32[]{:S(2)}) copy-start(f32[512]{0:T(512)} %param.27) | copy-start | bytes 6148
  106.5 32.0 %copy-start.2 = (bf16[2048,2]{0,1:T(2,128)(2,1)S(1)}, bf16[2048,2]{0,1:T(2,128)(2,1)}, u32[]{:S(2)}) copy-start(bf16[2048,2]{0,1:T(2,128)(2,1)} %param.24) | copy-start | bytes 24580
  106.5 32.0 %copy-start.3 = (bf16[2048,2]{0,1:T(2,128)(2,1)S(1)}, bf16[2048,2]{0,1:T(2,128)(2,1)}, u32[]{:S(2)}) copy-start(bf16[2048,2]{0,1:T(2,128)(2,1)} %param.23) | copy-start | bytes 24580
  110.8 121.2 %all-gather.11.cloned.1.call-start = ((), (), s32[]{:S(2)}) async-start(), calls=%async_computation.5 | async-start | bytes 1179648 | tf_op jit(solution)/shard_map/all_gather | solution.py:332
  148.8 41.8 %copy-start.8 = (f32[256]{0:T(256)S(1)}, f32[256]{0:T(256)}, u32[]{:S(2)}) copy-start(f32[256]{0:T(256)} %param.19) | copy-start | bytes 3076
  149.7 84.1 %copy-start.1 = (bf16[256,256]{1,0:T(8,128)(2,1)S(1)}, bf16[256,256]{1,0:T(8,128)(2,1)}, u32[]{:S(2)}) copy-start(bf16[256,256]{1,0:T(8,128)(2,1)} %param.28) | copy-start | bytes 393220
Sparse Core Ops, SparseCore 0:
  17.1 89.3 all-gather.6
  110.9 34.2 all-gather.8
  190.7 41.2 all-gather.10

commit v2 on v1

--- a/solution.py
+++ b/solution.py
@@ -1,6 +1,8 @@
 import jax
 import jax.numpy as jnp
 from jax import lax
+from jax.experimental import pallas as pl
+from jax.experimental.pallas import tpu as pltpu
 from jax.sharding import PartitionSpec as P
 
 BLOCK = 64
@@ -213,19 +215,448 @@
     return jnp.cumsum(coarse, axis=-1), jnp.cumsum(forget_log - coarse, axis=-1)
 
 
-def exchange_weights(pieces):
-    return lax.all_to_all(pieces, "sp", 0, 0, tiled=False)
-
-
-def gather_tokens(tokens):
-    whole = lax.all_gather(tokens, "tp", axis=1, tiled=True)
-    return lax.all_gather(whole, "sp", axis=0, tiled=True)
-
-
-def gather_in_group(mine, size):
-    count = lax.axis_size("sp")
-    groups = [list(range(first, first + size)) for first in range(0, count, size)]
-    return lax.all_gather(mine, "sp", axis_index_groups=groups)
+MESH = pl.DeviceIdType.MESH
+IN_VMEM = pl.BlockSpec(memory_space=pltpu.VMEM)
+ROLES = 4
+
+
+class Sends:
+    def __init__(self, semaphores):
+        self.semaphores = semaphores
+        self.started = []
+
+    def start(self, source, target, arrival, device, *conditions):
+        semaphore = self.semaphores.at[len(self.started)]
+        copy = pltpu.make_async_remote_copy(
+            src_ref=source,
+            dst_ref=target,
+            send_sem=semaphore,
+            recv_sem=arrival,
+            device_id=device,
+            device_id_type=MESH,
+        )
+        self.started.append((copy, conditions))
+        when(conditions, copy.start)
+
+    def finish(self):
+        for copy, conditions in self.started:
+            when(conditions, copy.wait_send)
+
+
+def when(conditions, action):
+    if not conditions:
+        action()
+        return
+    every = conditions[0]
+    for condition in conditions[1:]:
+        every = jnp.logical_and(every, condition)
+    pl.when(every)(action)
+
+
+def arrived(block, semaphore, *conditions):
+    copy = pltpu.make_async_remote_copy(
+        src_ref=block,
+        dst_ref=block,
+        send_sem=semaphore,
+        recv_sem=semaphore,
+        device_id=(lax.axis_index("sp"), lax.axis_index("tp")),
+        device_id_type=MESH,
+    )
+    when(conditions, copy.wait_recv)
+
+
+def line_order(here, count):
+    order = []
+    for distance in range(1, count):
+        order.append((here - distance, here >= distance, here + 1, here + 1 < count))
+        order.append((here + distance, here + distance < count, here - 1, here > 0))
+    return order
+
+
+def project_kernel(
+    count,
+    columns,
+    tokens,
+    wq,
+    wk,
+    wv,
+    wcv,
+    wcg,
+    gate_weights,
+    flat,
+    gates,
+    query,
+    key,
+    value,
+    whole,
+    weights,
+    mine,
+    send_sem,
+    token_sem,
+    weight_sem,
+    half_sem,
+    group_sem,
+):
+    me, tp = lax.axis_index("sp"), lax.axis_index("tp")
+    layers = count // 2
+    z, x, y, core = me // 2, lax.rem(me, 2), tp // 2, lax.rem(tp, 2)
+    length, features = tokens.shape
+    depth = wq.shape[0]
+    wide = weights.shape[1]
+    narrow = wide // 2
+    barrier = pltpu.get_barrier_semaphore()
+    y_side, core_side = (1 - y) * 2 + core, y * 2 + 1 - core
+    for step in range(1, count):
+        pl.semaphore_signal(
+            barrier, inc=1, device_id=(lax.rem(me + step, count), tp), device_id_type=MESH
+        )
+    for side in (y_side, core_side):
+        pl.semaphore_signal(barrier, inc=1, device_id=(me, side), device_id_type=MESH)
+
+    def block(i, j):
+        return whole.at[
+            pl.ds(pl.multiple_of(i * length, length), length),
+            pl.ds(pl.multiple_of(j * features, features), features),
+        ]
+
+    whole[
+        pl.ds(pl.multiple_of(me * length, length), length),
+        pl.ds(pl.multiple_of(tp * features, features), features),
+    ] = tokens[...]
+    sends = Sends(send_sem)
+    rows = pl.ds(pl.multiple_of(me * depth, depth), depth)
+    pl.semaphore_wait(barrier, count + 1)
+
+    def pass_on(i, j, source, sides, *conditions):
+        for device in sides:
+            sends.start(source, block(i, j), token_sem.at[i, j], device, *conditions)
+
+    x_side = z * 2 + 1 - x
+    sends.start(tokens, block(me, tp), token_sem.at[me, tp], (me - 2, tp), z > 0)
+    sends.start(tokens, block(me, tp), token_sem.at[me, tp], (me + 2, tp), z + 1 < layers)
+    pass_on(me, tp, tokens, ((x_side, tp), (me, y_side), (me, core_side)))
+    for target in range(count):
+        head, role = target // ROLES, target % ROLES
+        away = me != target
+        if role < 3:
+            window = (wq, wk, wv)[role].at[:, head * wide : (head + 1) * wide]
+            sends.start(window, weights.at[rows, :], weight_sem.at[me], (target, tp), away)
+
+            @pl.when(me == target)
+            def _():
+                weights[rows, :] = window[...]
+        else:
+            for side, (source, semaphore) in enumerate(((wcv, weight_sem), (wcg, half_sem))):
+                window = source.at[:, head * narrow : (head + 1) * narrow]
+                place = weights.at[rows, side * narrow : (side + 1) * narrow]
+                sends.start(window, place, semaphore.at[me], (target, tp), away)
+
+                @pl.when(me == target)
+                def _():
+                    place[...] = window[...]
+
+    order = line_order(z, layers)
+    for source, there, onward, further in order:
+        i = source * 2 + x
+        arrived(block(i, tp), token_sem.at[i, tp], there)
+        sends.start(
+            block(i, tp), block(i, tp), token_sem.at[i, tp], (onward * 2 + x, tp), there, further
+        )
+        pass_on(i, tp, block(i, tp), ((x_side, tp), (me, y_side), (me, core_side)), there)
+    for source, there in [(z, None)] + [entry[:2] for entry in order]:
+        conditions = () if there is None else (there,)
+        i = source * 2 + 1 - x
+        arrived(block(i, tp), token_sem.at[i, tp], *conditions)
+        pass_on(i, tp, block(i, tp), ((me, y_side), (me, core_side)), *conditions)
+    for step in range(count):
+        i = lax.rem(me + step, count)
+        arrived(block(i, y_side), token_sem.at[i, y_side])
+        pass_on(i, y_side, block(i, y_side), ((me, core_side),))
+    for step in range(count):
+        i = lax.rem(me + step, count)
+        for j in (core_side, (1 - y) * 2 + 1 - core):
+            arrived(block(i, j), token_sem.at[i, j])
+    role_here = lax.rem(me, ROLES)
+    for step in range(1, count):
+        i = lax.rem(me + step, count)
+        part = pl.ds(pl.multiple_of(i * depth, depth), depth)
+        arrived(weights.at[part, :], weight_sem.at[i], role_here < 3)
+        arrived(weights.at[part, :narrow], weight_sem.at[i], role_here == 3)
+        arrived(weights.at[part, narrow:], half_sem.at[i], role_here == 3)
+
+    total = flat.shape[0]
+    chunk = total // ROLES
+    for index in range(ROLES):
+        part = slice(index * chunk, (index + 1) * chunk)
+        lines = whole[part, :]
+        product = jnp.dot(lines, weights[...], preferred_element_type=jnp.float32)
+        flat[part, :] = product
+        mine[part, :] = product.astype(jnp.bfloat16)
+        gates[part, :] = jnp.dot(lines, gate_weights[...], preferred_element_type=jnp.float32)
+
+    first = me - role_here
+    for role in range(ROLES):
+        part = slice(role * chunk, (role + 1) * chunk)
+        until = slice(0, (role + 1) * chunk)
+        device = (first + role, tp)
+        for sender, target, source in (
+            (2, value.at[until, :], mine.at[until, :]),
+            (1, key.at[until, :], mine.at[until, :]),
+            (0, query, mine.at[part, :]),
+        ):
+            if sender != role:
+                sends.start(source, target, group_sem.at[sender], device, role_here == sender)
+            else:
+
+                @pl.when(role_here == role)
+                def _():
+                    target[...] = source[...]
+
+        @pl.when(role_here == role)
+        def _():
+            if (role + 1) * chunk < total:
+                rest = slice((role + 1) * chunk, total)
+                key[rest, :] = jnp.zeros_like(key[rest, :])
+                value[rest, :] = jnp.zeros_like(value[rest, :])
+
+    for role in range(ROLES):
+        until = slice(0, (role + 1) * chunk)
+        for sender, target in ((0, query), (1, key.at[until, :]), (2, value.at[until, :])):
+            if sender != role:
+                arrived(target, group_sem.at[sender], role_here == role)
+    sends.finish()
+
+
+def project(tokens, wq, wk, wv, wcv, wcg, gate_weights, head_dim):
+    count, columns = lax.axis_size("sp"), lax.axis_size("tp")
+    length, features = tokens.shape
+    total = length * count
+    f32, bf16 = jnp.float32, jnp.bfloat16
+    shape = jax.ShapeDtypeStruct
+    return pl.pallas_call(
+        lambda *refs: project_kernel(count, columns, *refs),
+        out_shape=(
+            shape((total, head_dim), f32),
+            shape((total, gate_weights.shape[1]), f32),
+            shape((total // ROLES, head_dim), bf16),
+            shape((total, head_dim), bf16),
+            shape((total, head_dim), bf16),
+        ),
+        in_specs=[IN_VMEM] * 7,
+        out_specs=(IN_VMEM,) * 5,
+        scratch_shapes=[
+            pltpu.VMEM((total, features * columns), bf16),
+            pltpu.VMEM((wq.shape[0] * count, head_dim), bf16),
+            pltpu.VMEM((total, head_dim), bf16),
+            pltpu.SemaphoreType.DMA((128,)),
+            pltpu.SemaphoreType.DMA((count, columns)),
+            pltpu.SemaphoreType.DMA((count,)),
+            pltpu.SemaphoreType.DMA((count,)),
+            pltpu.SemaphoreType.DMA((3,)),
+        ],
+        compiler_params=pltpu.CompilerParams(collective_id=0, has_side_effects=True),
+    )(tokens, wq, wk, wv, wcv, wcg, gate_weights)
+
+
+def sums_kernel(count, columns, sums, total, slots, send_sem, arrival_sem):
+    me, tp = lax.axis_index("sp"), lax.axis_index("tp")
+    groups = count // ROLES
+    members = groups * columns
+    role = lax.rem(me, ROLES)
+    own = (me // ROLES) * columns + tp
+    barrier = pltpu.get_barrier_semaphore()
+    peers = [lax.rem(own + step, members) for step in range(1, members)]
+    devices = [((peer // columns) * ROLES + role, lax.rem(peer, columns)) for peer in peers]
+    for device in devices:
+        pl.semaphore_signal(barrier, inc=1, device_id=device, device_id_type=MESH)
+    pl.semaphore_wait(barrier, members - 1)
+    sends = Sends(send_sem)
+    for device in devices:
+        sends.start(sums, slots.at[own], arrival_sem.at[own], device)
+    slots[own] = sums[...]
+    for peer in peers:
+        arrived(slots.at[peer], arrival_sem.at[peer])
+    result = slots[0]
+    for index in range(1, members):
+        result = result + slots[index]
+    total[...] = result
+    sends.finish()
+
+
+def sum_over_group(sums):
+    count, columns = lax.axis_size("sp"), lax.axis_size("tp")
+    members = count // ROLES * columns
+    return pl.pallas_call(
+        lambda *refs: sums_kernel(count, columns, *refs),
+        out_shape=jax.ShapeDtypeStruct(sums.shape, sums.dtype),
+        in_specs=[IN_VMEM],
+        out_specs=IN_VMEM,
+        scratch_shapes=[
+            pltpu.VMEM((members,) + sums.shape, sums.dtype),
+            pltpu.SemaphoreType.DMA((members,)),
+            pltpu.SemaphoreType.DMA((members,)),
+        ],
+        compiler_params=pltpu.CompilerParams(collective_id=1, has_side_effects=True),
+    )(sums)
+
+
+def mix_kernel(
+    count,
+    columns,
+    memory,
+    conv,
+    memory_weight,
+    conv_weight,
+    mixed,
+    memories,
+    convs,
+    partial,
+    slots,
+    send_sem,
+    memory_sem,
+    conv_sem,
+    slot_sem,
+):
+    me, tp = lax.axis_index("sp"), lax.axis_index("tp")
+    layers = count // 2
+    z, x = me // 2, lax.rem(me, 2)
+    chunk = memory.shape[0]
+    share = count // columns
+    barrier = pltpu.get_barrier_semaphore()
+    for step in range(1, count):
+        pl.semaphore_signal(
+            barrier, inc=1, device_id=(lax.rem(me + step, count), tp), device_id_type=MESH
+        )
+    inside = me // share == tp
+    for half in range(share):
+        for j in range(columns):
+            source = tp * share + half
+
+            @pl.when(tp != j)
+            def _():
+                pl.semaphore_signal(barrier, inc=1, device_id=(source, j), device_id_type=MESH)
+
+    @pl.when(inside)
+    def _():
+        pl.semaphore_wait(barrier, count - 1)
+
+    @pl.when(jnp.logical_not(inside))
+    def _():
+        pl.semaphore_wait(barrier, 2 * count - 1)
+
+    def memory_at(i):
+        rows = pl.multiple_of(lax.rem(i, ROLES) * chunk, chunk)
+        return memories.at[i // ROLES, pl.ds(rows, chunk), :]
+
+    def has_conv(i):
+        return lax.rem(i, ROLES) == ROLES - 1
+
+    sends = Sends(send_sem)
+
+    def spread(i, own, device, *conditions):
+        sends.start(
+            memory if own else memory_at(i), memory_at(i), memory_sem.at[i], device, *conditions
+        )
+        place = convs.at[i // ROLES]
+        sends.start(
+            conv if own else place, place, conv_sem.at[i], device, has_conv(i), *conditions
+        )
+
+    def received(i, *conditions):
+        arrived(memory_at(i), memory_sem.at[i], *conditions)
+        arrived(convs.at[i // ROLES], conv_sem.at[i], has_conv(i), *conditions)
+
+    x_side = (z * 2 + 1 - x, tp)
+    spread(me, True, (me - 2, tp), z > 0)
+    spread(me, True, (me + 2, tp), z + 1 < layers)
+    spread(me, True, x_side)
+    rows_here = pl.multiple_of(lax.rem(me, ROLES) * chunk, chunk)
+    memories[me // ROLES, pl.ds(rows_here, chunk), :] = memory[...]
+
+    @pl.when(has_conv(me))
+    def _():
+        convs[me // ROLES] = conv[...]
+
+    order = line_order(z, layers)
+    for source, there, onward, further in order:
+        i = source * 2 + x
+        received(i, there)
+        spread(i, False, (onward * 2 + x, tp), there, further)
+        spread(i, False, x_side, there)
+    received(z * 2 + 1 - x)
+    for source, there, _, _ in order:
+        received(source * 2 + 1 - x, there)
+
+    groups = count // ROLES
+    head_dim = memory.shape[1]
+    channels = conv.shape[1]
+    length = mixed.shape[0]
+    for index in range(ROLES):
+        part = slice(index * chunk, (index + 1) * chunk)
+        total = None
+        for head in range(groups):
+            term = jnp.dot(
+                memories[head, part, :],
+                memory_weight[head * head_dim : (head + 1) * head_dim, :],
+                preferred_element_type=jnp.float32,
+            ) + jnp.dot(
+                convs[head, part, :],
+                conv_weight[head * channels : (head + 1) * channels, :],
+                preferred_element_type=jnp.float32,
+            )
+            total = term if total is None else total + term
+        partial[part, :] = total.astype(jnp.bfloat16)
+        for i in range(index * chunk // length, (index + 1) * chunk // length):
+            column, half = me // share, lax.rem(me, share)
+            block = partial.at[i * length : (i + 1) * length, :]
+            away = jnp.logical_or(i != me, tp != column)
+            sends.start(block, slots.at[half, tp], slot_sem.at[half, tp], (i, column), away)
+
+            @pl.when(jnp.logical_not(away))
+            def _():
+                slots[half, tp] = block[...]
+
+    width = partial.shape[1]
+    for half in range(share):
+        total = None
+        for j in range(columns):
+            arrived(
+                slots.at[half, j],
+                slot_sem.at[half, j],
+                jnp.logical_or(tp * share + half != me, tp != j),
+            )
+        for j in range(columns):
+            term = slots[half, j].astype(jnp.float32)
+            total = term if total is None else total + term
+        mixed[:, half * width : (half + 1) * width] = total.astype(jnp.bfloat16)
+    sends.finish()
+
+
+def mix(memory, conv, memory_weight, conv_weight):
+    count, columns = lax.axis_size("sp"), lax.axis_size("tp")
+    chunk, head_dim = memory.shape
+    total, channels = conv.shape
+    groups, share = count // ROLES, count // columns
+    width = memory_weight.shape[1]
+    length = total // count
+    bf16 = jnp.bfloat16
+    return pl.pallas_call(
+        lambda *refs: mix_kernel(count, columns, *refs),
+        out_shape=jax.ShapeDtypeStruct((length, width * share), bf16),
+        in_specs=[IN_VMEM] * 4,
+        out_specs=IN_VMEM,
+        scratch_shapes=[
+            pltpu.VMEM((groups, total, head_dim), bf16),
+            pltpu.VMEM((groups, total, channels), bf16),
+            pltpu.VMEM((total, width), bf16),
+            pltpu.VMEM((share, columns, length, width), bf16),
+            pltpu.SemaphoreType.DMA((64,)),
+            pltpu.SemaphoreType.DMA((count,)),
+            pltpu.SemaphoreType.DMA((count,)),
+            pltpu.SemaphoreType.DMA((share, columns)),
+        ],
+        compiler_params=pltpu.CompilerParams(collective_id=2, has_side_effects=True),
+    )(memory, conv, memory_weight, conv_weight)
 
 
 def on_device_by_column(
@@ -250,40 +681,33 @@
     columns = lax.axis_size("tp")
     place = lax.axis_index("sp")
     heads_here = input_gate_weight.shape[1]
-    size = count // heads_here
-    head, quarter = place // size, place % size
-    depth = query_weight.shape[0]
+    head, role = place // ROLES, place % ROLES
     head_dim = query_weight.shape[1] // heads_here
-    slab = head_dim // size
-    channels = conv_value_weight.shape[1] // count
-    pieces = jnp.concatenate(
-        [
-            w.reshape(depth, count, -1)
-            for w in (query_weight, key_weight, value_weight, conv_value_weight, conv_gate_weight)
-        ],
-        axis=2,
-    ).transpose(1, 0, 2)
-    weights = exchange_weights(pieces).reshape(count * depth, -1)
-    whole = gather_tokens(tokens)
-    length = whole.shape[0]
+    channels = conv_value_weight.shape[1] // heads_here
+    gate_weights = jnp.concatenate([input_gate_weight, forget_gate_weight], axis=1)
+    flat, gates, query, key, value = project(
+        tokens,
+        query_weight,
+        key_weight,
+        value_weight,
+        conv_value_weight,
+        conv_gate_weight,
+        jnp.pad(gate_weights, ((0, 0), (0, 128 - 2 * heads_here))),
+        head_dim,
+    )
+    length = flat.shape[0]
     offsets = lax.all_gather(
         jnp.concatenate([input_offset, forget_offset], axis=1), "sp", axis=0, tiled=True
     )
-    gate_weights = jnp.concatenate([input_gate_weight, forget_gate_weight], axis=1)
-    flat = jnp.dot(whole, weights, preferred_element_type=f32)
-    gates = (jnp.dot(whole, gate_weights, preferred_element_type=f32) + offsets).T
-    glu = (
-        flat[:, 3 * slab : 3 * slab + channels] * jax.nn.sigmoid(flat[:, 3 * slab + channels :])
-    ).astype(bf16)
-    parts = gather_in_group(flat[:, : 3 * slab].astype(bf16), size)
-
+    gates = (gates[:, : 2 * heads_here] + offsets).T
+    glu = (flat[:, :channels] * jax.nn.sigmoid(flat[:, channels:])).astype(bf16)
     taps = conv_kernel.shape[0]
-    kernel = lax.dynamic_slice_in_dim(conv_kernel, place * channels, channels, 1).astype(f32)
+    kernel = lax.dynamic_slice_in_dim(conv_kernel, head * channels, channels, 1).astype(f32)
     extended = jnp.concatenate([jnp.zeros((taps - 1, channels), f32), glu.astype(f32)], axis=0)
     conv = depthwise(extended, kernel)
 
-    rows = length // size
-    start = quarter * rows
+    rows = length // ROLES
+    start = role * rows
     gate_in = lax.dynamic_index_in_dim(gates[:heads_here], head, 0, False)
     forget_log = jax.nn.log_sigmoid(
         lax.dynamic_index_in_dim(gates[heads_here:], head, 0, False)
@@ -299,10 +723,6 @@
     causal = (start + jnp.arange(rows))[:, None] >= jnp.arange(length)[None, :]
     log_weight = jnp.where(causal, log_weight, -jnp.inf)
     weight = jnp.exp(log_weight - jnp.max(log_weight, axis=1, keepdims=True))
-    query = lax.dynamic_slice_in_dim(parts[:, :, :slab], start, rows, 1)
-    query = query.transpose(1, 0, 2).reshape(rows, head_dim)
-    key = parts[:, :, slab : 2 * slab].transpose(1, 0, 2).reshape(length, head_dim)
-    value = parts[:, :, 2 * slab :].transpose(1, 0, 2).reshape(length, head_dim)
     scores = jnp.einsum("td,sd->ts", query, key, preferred_element_type=f32) * (
         weight * head_dim ** (-0.5)
     )
@@ -310,59 +730,45 @@
     denom = jnp.sum(scores, axis=1)
     cell = numer / jnp.maximum(jnp.abs(denom), 1.0)[:, None]
 
-    squares = lax.dynamic_update_slice_in_dim(
-        jnp.zeros((length,), f32), jnp.sum(cell * cell, axis=1), start, 0
-    )
-    sums = lax.psum(
-        jnp.stack([jnp.sum(conv, axis=1), jnp.sum(conv * conv, axis=1), squares]), ("sp", "tp")
-    )
-    total = channels * count * columns
+    squares = jnp.pad(jnp.sum(cell * cell, axis=1), (0, length - rows))
+    normed = role == ROLES - 1
+    sums = jnp.stack(
+        [
+            jnp.where(normed, jnp.sum(conv, axis=1), 0.0),
+            jnp.where(normed, jnp.sum(conv * conv, axis=1), 0.0),
+            squares,
+        ]
+    )
+    sums = sum_over_group(jnp.pad(sums, ((0, 5), (0, 0))))
+    total = conv_norm_gain.shape[0] * columns
     mean = sums[0] / total
     variance = sums[1] / total - mean * mean
-    gain = lax.dynamic_slice_in_dim(conv_norm_gain, place * channels, channels)
+    gain = lax.dynamic_slice_in_dim(conv_norm_gain, head * channels, channels)
     conv_branch = jax.nn.silu(
         (conv - mean[:, None]) * lax.rsqrt(variance + EPS)[:, None] * gain
     ).astype(bf16)
     entries = heads_here * head_dim * columns
-    memory_scale = lax.rsqrt(lax.dynamic_slice_in_dim(sums[2], start, rows) / entries + EPS)
+    memory_scale = lax.rsqrt(sums[2, :rows] / entries + EPS)
     memory_gain = lax.dynamic_slice_in_dim(memory_norm_gain, head * head_dim, head_dim)
     memory_branch = (cell * memory_scale[:, None] * memory_gain).astype(bf16)
 
-    conv_all = lax.all_gather(conv_branch, "sp")
-    memory_all = lax.all_gather(memory_branch, "sp")
-    conv_all = conv_all.transpose(1, 0, 2).reshape(length, -1)
-    memory_all = (
-        memory_all.reshape(heads_here, length, head_dim).transpose(1, 0, 2).reshape(length, -1)
-    )
-    partial = (
-        jnp.dot(conv_all, conv_out_weight, preferred_element_type=f32)
-        + jnp.dot(memory_all, memory_out_weight, preferred_element_type=f32)
-    ).astype(bf16)
-    return send_partials(partial)
-
-
-def send_partials(partial):
-    count, columns = lax.axis_size("sp"), lax.axis_size("tp")
-    length, width = partial.shape
-    swapped = lax.all_to_all(partial.reshape(count, length // count, width), "sp", 0, 0)
-    swapped = swapped.reshape(columns, count // columns, length // count, width)
-    groups = lax.all_to_all(swapped, "tp", 0, 0)
-    summed = jnp.sum(groups.astype(jnp.float32), axis=0).astype(jnp.bfloat16)
-    return summed.transpose(1, 0, 2).reshape(length // count, -1)
+    return mix(memory_branch, conv_branch, memory_out_weight, conv_out_weight)
 
 
 def splits_by_column(mesh, tokens, query_weight, conv_value_weight, input_gate_weight):
     count, columns = mesh.shape["sp"], mesh.shape["tp"]
-    heads_here = input_gate_weight.shape[1] // columns
-    head_dim = query_weight.shape[1] // input_gate_weight.shape[1]
-    if count % heads_here or count % columns:
-        return False
-    size = count // heads_here
+    heads = input_gate_weight.shape[1]
+    heads_here = heads // columns
+    head_dim = query_weight.shape[1] // heads
     return (
-        tokens.size * 2 <= 8 * 2**20
-        and head_dim % size == 0
-        and tokens.shape[0] % (size * 8) == 0
-        and conv_value_weight.shape[1] % (count * columns) == 0
+        count == ROLES * heads_here
+        and columns == 4
+        and count % columns == 0
+        and tokens.size * 2 <= 8 * 2**20
+        and tokens.shape[0] % (count * 16) == 0
+        and conv_value_weight.shape[1] * 2 == head_dim * heads
+        and head_dim % 256 == 0
+        and 2 * heads_here <= 128
     )
 
 

time: 271 us -> 196 us (0.72)
  Pallas kernels: 0 us -> 139 us
  blocking collectives: 138 us -> 38.8 us
  waiting for transfers between devices: 83.9 us -> 0 us
  between operations: 13.5 us -> 0.23 us
  local copies, waits for them, and re-layouts: 16.7 us -> 6.98 us
  matrix products: 8.81 us -> 1.06 us
  other arithmetic: 3.6 us -> 9.8 us
  starting transfers between devices: 5.92 us -> 0 us
    pallas_call x0 -> x3, Pallas kernels: none -> 139 us  [the longest x1 68.9 us: project(): pl.pallas_call(lambda *refs: project_kernel(count, columns, *refs), out_s...]
    all_gather x3 -> x0, waiting for transfers between devices: 46.8 us -> none  [the longest x1 37.1 us: gather_tokens(): return lax.all_gather(whole, 'sp', axis=0, tiled=True)]
    all_gather x2 -> x0, blocking collectives: 42.2 us -> none  [the longest x1 31.8 us: on_device_by_column(): conv_all = lax.all_gather(conv_branch, 'sp')]
    psum x1 -> x0, blocking collectives: 39.6 us -> none  [on_device_by_column(): lax.psum(jnp.stack([jnp.sum(conv, axis=1), jnp.sum(conv * conv, axis=1),...]
    all_to_all x1 -> x0, waiting for transfers between devices: 37.1 us -> none  [exchange_weights(): return lax.all_to_all(pieces, 'sp', 0, 0, tiled=False)]
    all_to_all x2 -> x0, blocking collectives: 28.5 us -> none  [the longest x1 17.2 us: send_partials(): lax.all_to_all(partial.reshape(count, length // count, width), 'sp', 0, 0)]
    all_gather x1, blocking collectives: 27.4 us -> 38.8 us  [on_device_by_column(): lax.all_gather(jnp.concatenate([input_offset, forget_offset], axis=1), 's...]
    dot_general x4 -> x0, matrix products: 7.71 us -> none  [the longest x1 3.52 us: on_device_by_column(): flat = jnp.dot(whole, weights, preferred_element_type=f32)]
  transfers between devices with their start and end apart: 4 -> 0, of which waited for: 4 -> 0; matrix products, arithmetic and copies ran while one was open for 6% -> 0% of each run, Pallas kernels for 0% -> 0%
where the time goes in v2:
time: 196 us
  Pallas kernels  139 us (71%)
  blocking collectives  38.8 us (20%)
  other arithmetic  9.8 us (5%)
  local copies, waits for them, and re-layouts  6.98 us (4%)
    pallas_call x1, Pallas kernels, project(): pl.pallas_call(lambda *refs: project_kernel(count, columns, *refs), out_s...  68.9 us
    pallas_call x1, Pallas kernels, mix(): pl.pallas_call(lambda *refs: mix_kernel(count, columns, *refs), out_shape...  61.7 us
    all_gather x1, blocking collectives, on_device_by_column(): lax.all_gather(jnp.concatenate([input_offset, forget_offset], axis=1), 's...  38.8 us
    pallas_call x1, Pallas kernels, sum_over_group(): pl.pallas_call(lambda *refs: sums_kernel(count, columns, *refs), out_shap...  8.07 us
    unnamed x23, local copies, waits for them, and re-layouts  4.72 us

profile of v2, /device:TPU:0, one launch (start us, length us, event | category | flops | bytes accessed | tf_op | source)
XLA Modules:
  0.0 195.6 jit_solution(9056143821392558262)
XLA Ops:
  0.0 0.7 copy-done.3
  0.8 0.7 copy-done.2
  1.5 0.3 copy.26
  1.8 0.9 pad.13.refs_6_
  2.7 68.9 %shard_map.145 = (f32[1024,256]{1,0:T(8,128)}, f32[1024,128]{1,0:T(8,128)}, bf16[256,256]{1,0:T(8,128)(2,1)}, bf16[1024,256]{1,0:T(8,128)(2,1)}, bf16[1024,256]{1,0:T(8,128)(2,1)}) custom-call(bf16[128,512]{1,0:T(8,128)(2,1)} %refs_0_.1, bf16[256,512]{1,0:T(8,128)(2,1)} %refs_1_.1, bf16[256,512]{1,0:T(8,128)(2,1)} %refs_2_.2, bf16[256,512]{1,0:T(8,128)(2,1)} %refs_3_.2, ...), custom_call_target="tpu_custom_call" | custom-call | tf_op jit(solution)/shard_map/pallas_call | solution.py:436
  71.7 1.3 fusion.23
  73.1 2.4 %fusion.30 = (f32[1024]{0:T(1024)S(1)}, f32[1024]{0:T(1024)S(1)}, f32[1024,128]{1,0:T(8,128)S(1)}) fusion(f32[1024,128]{1,0:T(8,128)S(1)} %fusion.23, f32[128]{0:T(128)S(1)} %get-tuple-element.23, f32[128]{0:T(128)S(1)} %get-tuple-element.24, f32[128]{0:T(128)S(1)} %get-tuple-element.25, f32[128]{0:T(128)S(1)} %get-tuple-element.26, ...), kind=kLoop, calls=%fused_computation.107 | loop fusion | flops 8386560 | bytes 1072640 | tf_op jit(solution)/shard_map/reduce_sum | solution.py:737
  75.7 38.8 %all_gather.3 = f32[1024,4]{1,0:T(8,128)S(1)} all-gather(f32[128,4]{1,0:T(8,128)S(1)} %copy.27), channel_id=1, replica_groups=mesh['sp'=8,'tp'=4] {'sp'}, dimensions={0}, use_global_device_ids=true | all-gather | bytes 18432 | tf_op jit(solution)/shard_map/all_gather | solution.py:699
  114.8 0.6 dynamic-slice_reduce_fusion
  115.5 0.3 reduce-window.16
  116.8 0.5 fusion
  117.3 0.7 fusion.32
  118.0 0.3 copy-done.7
  118.3 0.4 multiply_reduce_fusion.1
  118.7 0.6 select_maximum_fusion.refs_0_
  119.4 8.1 %shard_map.146 = f32[8,1024]{1,0:T(8,128)} custom-call(f32[8,1024]{1,0:T(8,128)} %select_maximum_fusion.refs_0_), custom_call_target="tpu_custom_call" | custom-call | tf_op jit(solution)/shard_map/pallas_call | solution.py:489
  127.4 0.8 slice_multiply_fusion.1
  128.3 0.7 copy-done.10
  129.1 1.0 multiply_convert_fusion.refs_1_
  130.1 0.7 add_rsqrt_fusion.1
  130.8 0.7 copy-done.6
  131.6 0.8 multiply_convert_fusion.2.refs_0_
  132.3 61.7 %shard_map.147 = bf16[128,512]{1,0:T(8,128)(2,1)} custom-call(bf16[256,256]{1,0:T(8,128)(2,1)} %multiply_convert_fusion.2.refs_0_, bf16[1024,128]{1,0:T(8,128)(2,1)} %multiply_convert_fusion.refs_1_, bf16[512,256]{1,0:T(8,128)(2,1)} %refs_2_.3, bf16[256,256]{1,0:T(8,128)(2,1)} %refs_3_.3), custom_call_target="tpu_custom_call" | custom-call | tf_op jit(solution)/shard_map/pallas_call | solution.py:643
  194.0 1.6 copy.31
  (44 shorter events, 1.7 us)
Async XLA Ops:
  0.0 0.7 copy-start.3
  0.8 0.7 copy-start.2
  0.8 0.7 copy-start.1
  73.0 2.5 %copy-start.4 = (f32[128,2]{0,1:T(2,128)S(1)}, f32[128,2]{0,1:T(2,128)}, u32[]{:S(2)}) copy-start(f32[128,2]{0,1:T(2,128)} %param.26) | copy-start | bytes 3076
  73.0 2.5 %copy-start.5 = (f32[128,2]{0,1:T(2,128)S(1)}, f32[128,2]{0,1:T(2,128)}, u32[]{:S(2)}) copy-start(f32[128,2]{0,1:T(2,128)} %param.25) | copy-start | bytes 3076
  75.5 39.0 %copy-start = (f32[1024,128]{1,0:T(8,128)S(1)}, f32[1024,128]{1,0:T(8,128)}, u32[]{:S(2)}) copy-start(f32[1024,128]{1,0:T(8,128)} %get-tuple-element.12) | copy-start | bytes 1572868
  114.8 2.5 %copy-start.8 = (bf16[1024,256]{1,0:T(8,128)(2,1)S(1)}, bf16[1024,256]{1,0:T(8,128)(2,1)}, u32[]{:S(2)}) copy-start(bf16[1024,256]{1,0:T(8,128)(2,1)} %get-tuple-element.11) | copy-start | bytes 1572868
  115.5 1.8 copy-start.9
  117.3 1.0 copy-start.7
  128.3 0.7 copy-start.10
  130.8 0.7 copy-start.6

commit v3 on v2

--- a/solution.py
+++ b/solution.py
@@ -265,6 +265,11 @@
     when(conditions, copy.wait_recv)
 
 
+def role_of(i):
+    flip = lax.rem(i // ROLES, 2)
+    return lax.rem(i, ROLES) + flip * (1 - 2 * lax.rem(i, 2))
+
+
 def line_order(here, count):
     order = []
     for distance in range(1, count):
@@ -283,11 +288,13 @@
     wcv,
     wcg,
     gate_weights,
+    own_offsets,
     flat,
     gates,
     query,
     key,
     value,
+    offsets,
     whole,
     weights,
     mine,
@@ -296,6 +303,7 @@
     weight_sem,
     half_sem,
     group_sem,
+    offset_sem,
 ):
     me, tp = lax.axis_index("sp"), lax.axis_index("tp")
     layers = count // 2
@@ -335,28 +343,36 @@
     sends.start(tokens, block(me, tp), token_sem.at[me, tp], (me - 2, tp), z > 0)
     sends.start(tokens, block(me, tp), token_sem.at[me, tp], (me + 2, tp), z + 1 < layers)
     pass_on(me, tp, tokens, ((x_side, tp), (me, y_side), (me, core_side)))
-    for target in range(count):
-        head, role = target // ROLES, target % ROLES
-        away = me != target
-        if role < 3:
-            window = (wq, wk, wv)[role].at[:, head * wide : (head + 1) * wide]
-            sends.start(window, weights.at[rows, :], weight_sem.at[me], (target, tp), away)
-
-            @pl.when(me == target)
-            def _():
-                weights[rows, :] = window[...]
-        else:
-            for side, (source, semaphore) in enumerate(((wcv, weight_sem), (wcg, half_sem))):
-                window = source.at[:, head * narrow : (head + 1) * narrow]
-                place = weights.at[rows, side * narrow : (side + 1) * narrow]
-                sends.start(window, place, semaphore.at[me], (target, tp), away)
+    for step in range(1, count):
+        device = (lax.rem(me + step, count), tp)
+        sends.start(own_offsets, offsets.at[me], offset_sem.at[me], device)
+    offsets[me] = own_offsets[...]
+
+    def send_weights():
+        for target in range(count):
+            head, role = target // ROLES, (target % ROLES) ^ (target // ROLES % 2)
+            away = me != target
+            if role < 3:
+                window = (wq, wk, wv)[role].at[:, head * wide : (head + 1) * wide]
+                sends.start(window, weights.at[rows, :], weight_sem.at[me], (target, tp), away)
 
                 @pl.when(me == target)
                 def _():
-                    place[...] = window[...]
+                    weights[rows, :] = window[...]
+            else:
+                for side, (source, semaphore) in enumerate(((wcv, weight_sem), (wcg, half_sem))):
+                    window = source.at[:, head * narrow : (head + 1) * narrow]
+                    place = weights.at[rows, side * narrow : (side + 1) * narrow]
+                    sends.start(window, place, semaphore.at[me], (target, tp), away)
+
+                    @pl.when(me == target)
+                    def _():
+                        place[...] = window[...]
 
     order = line_order(z, layers)
-    for source, there, onward, further in order:
+    for index, (source, there, onward, further) in enumerate(order):
+        if index == 2:
+            send_weights()
         i = source * 2 + x
         arrived(block(i, tp), token_sem.at[i, tp], there)
         sends.start(
@@ -376,9 +392,10 @@
         i = lax.rem(me + step, count)
         for j in (core_side, (1 - y) * 2 + 1 - core):
             arrived(block(i, j), token_sem.at[i, j])
-    role_here = lax.rem(me, ROLES)
+    role_here = role_of(me)
     for step in range(1, count):
         i = lax.rem(me + step, count)
+        arrived(offsets.at[i], offset_sem.at[i])
         part = pl.ds(pl.multiple_of(i * depth, depth), depth)
         arrived(weights.at[part, :], weight_sem.at[i], role_here < 3)
         arrived(weights.at[part, :narrow], weight_sem.at[i], role_here == 3)
@@ -394,11 +411,12 @@
         mine[part, :] = product.astype(jnp.bfloat16)
         gates[part, :] = jnp.dot(lines, gate_weights[...], preferred_element_type=jnp.float32)
 
-    first = me - role_here
+    first = me - lax.rem(me, ROLES)
+    flip = lax.rem(me // ROLES, 2)
     for role in range(ROLES):
         part = slice(role * chunk, (role + 1) * chunk)
         until = slice(0, (role + 1) * chunk)
-        device = (first + role, tp)
+        device = (first + role + flip * (1 - 2 * (role % 2)), tp)
         for sender, target, source in (
             (2, value.at[until, :], mine.at[until, :]),
             (1, key.at[until, :], mine.at[until, :]),
@@ -427,7 +445,7 @@
     sends.finish()
 
 
-def project(tokens, wq, wk, wv, wcv, wcg, gate_weights, head_dim):
+def project(tokens, wq, wk, wv, wcv, wcg, gate_weights, own_offsets, head_dim):
     count, columns = lax.axis_size("sp"), lax.axis_size("tp")
     length, features = tokens.shape
     total = length * count
@@ -441,9 +459,10 @@
             shape((total // ROLES, head_dim), bf16),
             shape((total, head_dim), bf16),
             shape((total, head_dim), bf16),
+            shape((count,) + own_offsets.shape, f32),
         ),
-        in_specs=[IN_VMEM] * 7,
-        out_specs=(IN_VMEM,) * 5,
+        in_specs=[IN_VMEM] * 8,
+        out_specs=(IN_VMEM,) * 6,
         scratch_shapes=[
             pltpu.VMEM((total, features * columns), bf16),
             pltpu.VMEM((wq.shape[0] * count, head_dim), bf16),
@@ -453,20 +472,25 @@
             pltpu.SemaphoreType.DMA((count,)),
             pltpu.SemaphoreType.DMA((count,)),
             pltpu.SemaphoreType.DMA((3,)),
+            pltpu.SemaphoreType.DMA((count,)),
         ],
         compiler_params=pltpu.CompilerParams(collective_id=0, has_side_effects=True),
-    )(tokens, wq, wk, wv, wcv, wcg, gate_weights)
+    )(tokens, wq, wk, wv, wcv, wcg, gate_weights, own_offsets)
 
 
 def sums_kernel(count, columns, sums, total, slots, send_sem, arrival_sem):
     me, tp = lax.axis_index("sp"), lax.axis_index("tp")
     groups = count // ROLES
     members = groups * columns
-    role = lax.rem(me, ROLES)
+    role = role_of(me)
     own = (me // ROLES) * columns + tp
     barrier = pltpu.get_barrier_semaphore()
     peers = [lax.rem(own + step, members) for step in range(1, members)]
-    devices = [((peer // columns) * ROLES + role, lax.rem(peer, columns)) for peer in peers]
+    devices = []
+    for peer in peers:
+        group = peer // columns
+        seat = role + lax.rem(group, 2) * (1 - 2 * lax.rem(role, 2))
+        devices.append((group * ROLES + seat, lax.rem(peer, columns)))
     for device in devices:
         pl.semaphore_signal(barrier, inc=1, device_id=device, device_id_type=MESH)
     pl.semaphore_wait(barrier, members - 1)
@@ -545,11 +569,11 @@
         pl.semaphore_wait(barrier, 2 * count - 1)
 
     def memory_at(i):
-        rows = pl.multiple_of(lax.rem(i, ROLES) * chunk, chunk)
+        rows = pl.multiple_of(role_of(i) * chunk, chunk)
         return memories.at[i // ROLES, pl.ds(rows, chunk), :]
 
     def has_conv(i):
-        return lax.rem(i, ROLES) == ROLES - 1
+        return role_of(i) == ROLES - 1
 
     sends = Sends(send_sem)
 
@@ -570,7 +594,7 @@
     spread(me, True, (me - 2, tp), z > 0)
     spread(me, True, (me + 2, tp), z + 1 < layers)
     spread(me, True, x_side)
-    rows_here = pl.multiple_of(lax.rem(me, ROLES) * chunk, chunk)
+    rows_here = pl.multiple_of(role_of(me) * chunk, chunk)
     memories[me // ROLES, pl.ds(rows_here, chunk), :] = memory[...]
 
     @pl.when(has_conv(me))
@@ -681,11 +705,12 @@
     columns = lax.axis_size("tp")
     place = lax.axis_index("sp")
     heads_here = input_gate_weight.shape[1]
-    head, role = place // ROLES, place % ROLES
+    head, role = place // ROLES, role_of(place)
     head_dim = query_weight.shape[1] // heads_here
     channels = conv_value_weight.shape[1] // heads_here
     gate_weights = jnp.concatenate([input_gate_weight, forget_gate_weight], axis=1)
-    flat, gates, query, key, value = project(
+    own_offsets = jnp.concatenate([input_offset, forget_offset], axis=1).T
+    flat, gates, query, key, value, offsets = project(
         tokens,
         query_weight,
         key_weight,
@@ -693,13 +718,12 @@
         conv_value_weight,
         conv_gate_weight,
         jnp.pad(gate_weights, ((0, 0), (0, 128 - 2 * heads_here))),
+        jnp.pad(own_offsets, ((0, -2 * heads_here % 8), (0, 0))),
         head_dim,
     )
     length = flat.shape[0]
-    offsets = lax.all_gather(
-        jnp.concatenate([input_offset, forget_offset], axis=1), "sp", axis=0, tiled=True
-    )
-    gates = (gates[:, : 2 * heads_here] + offsets).T
+    offsets = offsets[:, : 2 * heads_here].transpose(1, 0, 2).reshape(2 * heads_here, length)
+    gates = gates[:, : 2 * heads_here].T + offsets
     glu = (flat[:, :channels] * jax.nn.sigmoid(flat[:, channels:])).astype(bf16)
     taps = conv_kernel.shape[0]
     kernel = lax.dynamic_slice_in_dim(conv_kernel, head * channels, channels, 1).astype(f32)

time: 196 us -> 165 us (0.84)
  blocking collectives: 38.8 us -> 0 us
  Pallas kernels: 139 us -> 144 us
    all_gather x1 -> x0, blocking collectives: 38.8 us -> none  [on_device_by_column(): lax.all_gather(jnp.concatenate([input_offset, forget_offset], axis=1), 's...]
    pallas_call x1, Pallas kernels: 61.7 us -> 71.5 us  [mix(): pl.pallas_call(lambda *refs: mix_kernel(count, columns, *refs), out_shape...]
    pallas_call x1, Pallas kernels: 68.9 us -> 63.8 us  [project(): pl.pallas_call(lambda *refs: project_kernel(count, columns, *refs), out_s...]
    unnamed x23 -> x25, local copies, waits for them, and re-layouts: 4.72 us -> 5.45 us
where the time goes in v3:
time: 165 us; the launch traced here: 163 us
  Pallas kernels  144 us (87%)
  other arithmetic  9.78 us (6%)
  local copies, waits for them, and re-layouts  8.42 us (5%)
    pallas_call x1, Pallas kernels, mix(): pl.pallas_call(lambda *refs: mix_kernel(count, columns, *refs), out_shape...  71.5 us
    pallas_call x1, Pallas kernels, project(): pl.pallas_call(lambda *refs: project_kernel(count, columns, *refs), out_s...  63.8 us
    pallas_call x1, Pallas kernels, sum_over_group(): pl.pallas_call(lambda *refs: sums_kernel(count, columns, *refs), out_shap...  8.54 us
    unnamed x25, local copies, waits for them, and re-layouts  5.45 us

profile of v3, /device:TPU:0, one launch (start us, length us, event | category | flops | bytes accessed | tf_op | source)
XLA Modules:
  0.0 163.4 jit_solution(7575574453089465389)
XLA Ops:
  0.0 0.7 copy-done.4
  0.8 0.7 copy-done.3
  1.5 0.3 copy.23
  1.8 0.9 pad.17.refs_6_
  2.8 0.6 pad.18.refs_7_
  3.4 63.8 %shard_map.145 = (f32[1024,256]{1,0:T(8,128)}, f32[1024,128]{1,0:T(8,128)}, bf16[256,256]{1,0:T(8,128)(2,1)}, bf16[1024,256]{1,0:T(8,128)(2,1)}, bf16[1024,256]{1,0:T(8,128)(2,1)}, /*index=5*/f32[8,8,128]{2,1,0:T(8,128)}) custom-call(bf16[128,512]{1,0:T(8,128)(2,1)} %refs_0_.1, bf16[256,512]{1,0:T(8,128)(2,1)} %refs_1_.1, bf16[256,512]{1,0:T(8,128)(2,1)} %refs_2_.2, ...), custom_call_target="tpu_custom_call" | custom-call | tf_op jit(solution)/shard_map/pallas_call | solution.py:454
  67.2 1.3 fusion.23
  68.6 2.4 %fusion.30 = (f32[1024]{0:T(1024)S(1)}, f32[1024]{0:T(1024)S(1)}, f32[1024,128]{1,0:T(8,128)S(1)}) fusion(f32[1024,128]{1,0:T(8,128)S(1)} %fusion.23, f32[128]{0:T(128)S(1)} %get-tuple-element.25, f32[128]{0:T(128)S(1)} %get-tuple-element.26, f32[128]{0:T(128)S(1)} %get-tuple-element.27, f32[128]{0:T(128)S(1)} %get-tuple-element.28, ...), kind=kLoop, calls=%fused_computation.108 | loop fusion | flops 8386560 | bytes 1072640 | tf_op jit(solution)/shard_map/reduce_sum | solution.py:761
  71.3 0.7 copy-done
  72.3 0.6 dynamic-slice_reduce_fusion
  74.3 0.5 fusion
  74.8 0.7 fusion.32
  75.5 0.3 copy-done.8
  75.8 0.4 multiply_reduce_fusion.1
  76.2 0.6 select_maximum_fusion.refs_0_
  76.9 8.5 %shard_map.146 = f32[8,1024]{1,0:T(8,128)} custom-call(f32[8,1024]{1,0:T(8,128)} %select_maximum_fusion.refs_0_), custom_call_target="tpu_custom_call" | custom-call | tf_op jit(solution)/shard_map/pallas_call | solution.py:513
  85.4 0.8 slice_multiply_fusion.1
  86.3 0.7 copy-done.11
  87.0 1.0 multiply_convert_fusion.refs_1_
  88.1 0.7 add_rsqrt_fusion.1
  88.8 0.7 copy-done.7
  89.6 0.8 multiply_convert_fusion.2.refs_0_
  90.3 71.5 %shard_map.147 = bf16[128,512]{1,0:T(8,128)(2,1)} custom-call(bf16[256,256]{1,0:T(8,128)(2,1)} %multiply_convert_fusion.2.refs_0_, bf16[1024,128]{1,0:T(8,128)(2,1)} %multiply_convert_fusion.refs_1_, bf16[512,256]{1,0:T(8,128)(2,1)} %refs_2_.3, bf16[256,256]{1,0:T(8,128)(2,1)} %refs_3_.3), custom_call_target="tpu_custom_call" | custom-call | tf_op jit(solution)/shard_map/pallas_call | solution.py:667
  161.9 1.6 copy.28
  (47 shorter events, 2.1 us)
Async XLA Ops:
  0.0 0.7 copy-start.4
  0.8 0.7 copy-start.3
  0.8 0.7 copy-start.2
  1.8 0.9 copy-start.5
  1.8 0.9 copy-start.6
  68.5 2.5 %copy-start.1 = (f32[8,8,128]{2,1,0:T(8,128)S(1)}, f32[8,8,128]{2,1,0:T(8,128)}, u32[]{:S(2)}) copy-start(f32[8,8,128]{2,1,0:T(8,128)} %get-tuple-element.14) | copy-start | bytes 98308
  71.0 1.0 copy-start
  72.3 2.5 %copy-start.9 = (bf16[1024,256]{1,0:T(8,128)(2,1)S(1)}, bf16[1024,256]{1,0:T(8,128)(2,1)}, u32[]{:S(2)}) copy-start(bf16[1024,256]{1,0:T(8,128)(2,1)} %get-tuple-element.12) | copy-start | bytes 1572868
  73.0 1.8 %copy-start.10 = (bf16[256,256]{1,0:T(8,128)(2,1)S(1)}, bf16[256,256]{1,0:T(8,128)(2,1)}, u32[]{:S(2)}) copy-start(bf16[256,256]{1,0:T(8,128)(2,1)} %get-tuple-element.11) | copy-start | bytes 393220
  74.8 1.0 copy-start.8
  86.3 0.7 copy-start.11
  88.8 0.7 copy-start.7

commit v4 on v3

--- a/solution.py
+++ b/solution.py
@@ -349,25 +349,34 @@
     offsets[me] = own_offsets[...]
 
     def send_weights():
-        for target in range(count):
-            head, role = target // ROLES, (target % ROLES) ^ (target // ROLES % 2)
-            away = me != target
+        for step in range(1, count):
+            target = lax.rem(me + step, count)
+            head, role = target // ROLES, role_of(target)
+            device = (target, tp)
+            window = pl.ds(pl.multiple_of(head * wide, wide), wide)
+            for index, source in enumerate((wq, wk, wv)):
+                sends.start(
+                    source.at[:, window],
+                    weights.at[rows, :],
+                    weight_sem.at[me],
+                    device,
+                    role == index,
+                )
+            window = pl.ds(pl.multiple_of(head * narrow, narrow), narrow)
+            for side, (source, semaphore) in enumerate(((wcv, weight_sem), (wcg, half_sem))):
+                place = weights.at[rows, side * narrow : (side + 1) * narrow]
+                sends.start(source.at[:, window], place, semaphore.at[me], device, role == 3)
+
+    for target in range(count):
+        head, role = target // ROLES, (target % ROLES) ^ (target // ROLES % 2)
+
+        @pl.when(me == target)
+        def _():
             if role < 3:
-                window = (wq, wk, wv)[role].at[:, head * wide : (head + 1) * wide]
-                sends.start(window, weights.at[rows, :], weight_sem.at[me], (target, tp), away)
-
-                @pl.when(me == target)
-                def _():
-                    weights[rows, :] = window[...]
+                weights[rows, :] = (wq, wk, wv)[role][:, head * wide : (head + 1) * wide]
             else:
-                for side, (source, semaphore) in enumerate(((wcv, weight_sem), (wcg, half_sem))):
-                    window = source.at[:, head * narrow : (head + 1) * narrow]
-                    place = weights.at[rows, side * narrow : (side + 1) * narrow]
-                    sends.start(window, place, semaphore.at[me], (target, tp), away)
-
-                    @pl.when(me == target)
-                    def _():
-                        place[...] = window[...]
+                weights[rows, :narrow] = wcv[:, head * narrow : (head + 1) * narrow]
+                weights[rows, narrow:] = wcg[:, head * narrow : (head + 1) * narrow]
 
     order = line_order(z, layers)
     for index, (source, there, onward, further) in enumerate(order):
@@ -467,7 +476,7 @@
             pltpu.VMEM((total, features * columns), bf16),
             pltpu.VMEM((wq.shape[0] * count, head_dim), bf16),
             pltpu.VMEM((total, head_dim), bf16),
-            pltpu.SemaphoreType.DMA((128,)),
+            pltpu.SemaphoreType.DMA((192,)),
             pltpu.SemaphoreType.DMA((count, columns)),
             pltpu.SemaphoreType.DMA((count,)),
             pltpu.SemaphoreType.DMA((count,)),
@@ -577,23 +586,38 @@
 
     sends = Sends(send_sem)
 
-    def spread(i, own, device, *conditions):
+    def piece(index):
+        return slice(index * chunk, (index + 1) * chunk)
+
+    def spread_memory(i, own, device, *conditions):
         sends.start(
             memory if own else memory_at(i), memory_at(i), memory_sem.at[i], device, *conditions
         )
-        place = convs.at[i // ROLES]
+
+    def spread_conv(i, index, own, device, *conditions):
+        place = convs.at[i // ROLES, piece(index), :]
         sends.start(
-            conv if own else place, place, conv_sem.at[i], device, has_conv(i), *conditions
+            conv.at[piece(index), :] if own else place,
+            place,
+            conv_sem.at[i, index],
+            device,
+            has_conv(i),
+            *conditions,
         )
 
-    def received(i, *conditions):
-        arrived(memory_at(i), memory_sem.at[i], *conditions)
-        arrived(convs.at[i // ROLES], conv_sem.at[i], has_conv(i), *conditions)
+    def conv_arrived(i, index, *conditions):
+        place = convs.at[i // ROLES, piece(index), :]
+        arrived(place, conv_sem.at[i, index], has_conv(i), *conditions)
 
     x_side = (z * 2 + 1 - x, tp)
-    spread(me, True, (me - 2, tp), z > 0)
-    spread(me, True, (me + 2, tp), z + 1 < layers)
-    spread(me, True, x_side)
+    below, above = (me - 2, tp), (me + 2, tp)
+    spread_memory(me, True, below, z > 0)
+    spread_memory(me, True, above, z + 1 < layers)
+    spread_memory(me, True, x_side)
+    for index in range(ROLES):
+        spread_conv(me, index, True, below, z > 0)
+        spread_conv(me, index, True, above, z + 1 < layers)
+        spread_conv(me, index, True, x_side)
     rows_here = pl.multiple_of(role_of(me) * chunk, chunk)
     memories[me // ROLES, pl.ds(rows_here, chunk), :] = memory[...]
 
@@ -604,12 +628,20 @@
     order = line_order(z, layers)
     for source, there, onward, further in order:
         i = source * 2 + x
-        received(i, there)
-        spread(i, False, (onward * 2 + x, tp), there, further)
-        spread(i, False, x_side, there)
-    received(z * 2 + 1 - x)
-    for source, there, _, _ in order:
-        received(source * 2 + 1 - x, there)
+        arrived(memory_at(i), memory_sem.at[i], there)
+        spread_memory(i, False, (onward * 2 + x, tp), there, further)
+        spread_memory(i, False, x_side, there)
+    for source, there, onward, further in order:
+        i = source * 2 + x
+        for index in range(ROLES):
+            conv_arrived(i, index, there)
+            spread_conv(i, index, False, (onward * 2 + x, tp), there, further)
+            spread_conv(i, index, False, x_side, there)
+    for source, there in [(z, z >= 0)] + [entry[:2] for entry in order]:
+        i = source * 2 + 1 - x
+        arrived(memory_at(i), memory_sem.at[i], there)
+        for index in range(ROLES):
+            conv_arrived(i, index, there)
 
     groups = count // ROLES
     head_dim = memory.shape[1]
@@ -630,15 +662,19 @@
             )
             total = term if total is None else total + term
         partial[part, :] = total.astype(jnp.bfloat16)
-        for i in range(index * chunk // length, (index + 1) * chunk // length):
-            column, half = me // share, lax.rem(me, share)
-            block = partial.at[i * length : (i + 1) * length, :]
-            away = jnp.logical_or(i != me, tp != column)
-            sends.start(block, slots.at[half, tp], slot_sem.at[half, tp], (i, column), away)
+    column, half = me // share, lax.rem(me, share)
+    for step in range(count):
+        i = lax.rem(me + step, count)
+        place = pl.ds(pl.multiple_of(i * length, length), length)
+        away = jnp.logical_or(i != me, tp != column)
+        sends.start(
+            partial.at[place, :], slots.at[half, tp], slot_sem.at[half, tp], (i, column), away
+        )
+        if step == 0:
 
             @pl.when(jnp.logical_not(away))
             def _():
-                slots[half, tp] = block[...]
+                slots[half, tp] = partial[place, :]
 
     width = partial.shape[1]
     for half in range(share):
@@ -674,9 +710,9 @@
             pltpu.VMEM((groups, total, channels), bf16),
             pltpu.VMEM((total, width), bf16),
             pltpu.VMEM((share, columns, length, width), bf16),
-            pltpu.SemaphoreType.DMA((64,)),
+            pltpu.SemaphoreType.DMA((96,)),
             pltpu.SemaphoreType.DMA((count,)),
-            pltpu.SemaphoreType.DMA((count,)),
+            pltpu.SemaphoreType.DMA((count, ROLES)),
             pltpu.SemaphoreType.DMA((share, columns)),
         ],
         compiler_params=pltpu.CompilerParams(collective_id=2, has_side_effects=True),

time: 165 us -> 153 us (0.927)
  Pallas kernels: 144 us -> 132 us
    pallas_call x1, Pallas kernels: 71.5 us -> 59.1 us  [mix(): pl.pallas_call(lambda *refs: mix_kernel(count, columns, *refs), out_shape...]
where the time goes in v4:
time: 153 us; the launch traced here: 152 us
  Pallas kernels  132 us (86%)
  other arithmetic  9.78 us (6%)
  local copies, waits for them, and re-layouts  8.42 us (6%)
    pallas_call x1, Pallas kernels, project(): pl.pallas_call(lambda *refs: project_kernel(count, columns, *refs), out_s...  64.4 us
    pallas_call x1, Pallas kernels, mix(): pl.pallas_call(lambda *refs: mix_kernel(count, columns, *refs), out_shape...  59.1 us
    pallas_call x1, Pallas kernels, sum_over_group(): pl.pallas_call(lambda *refs: sums_kernel(count, columns, *refs), out_shap...  8.54 us
    unnamed x25, local copies, waits for them, and re-layouts  5.45 us

profile of v4, /device:TPU:0, one launch (start us, length us, event | category | flops | bytes accessed | tf_op | source)
XLA Modules:
  0.0 151.6 jit_solution(9686636963165992315)
XLA Ops:
  0.0 0.7 copy-done.4
  0.8 0.7 copy-done.3
  1.5 0.3 copy.23
  1.8 0.9 pad.17.refs_6_
  2.8 0.6 pad.18.refs_7_
  3.4 64.4 %shard_map.145 = (f32[1024,256]{1,0:T(8,128)}, f32[1024,128]{1,0:T(8,128)}, bf16[256,256]{1,0:T(8,128)(2,1)}, bf16[1024,256]{1,0:T(8,128)(2,1)}, bf16[1024,256]{1,0:T(8,128)(2,1)}, /*index=5*/f32[8,8,128]{2,1,0:T(8,128)}) custom-call(bf16[128,512]{1,0:T(8,128)(2,1)} %refs_0_.1, bf16[256,512]{1,0:T(8,128)(2,1)} %refs_1_.1, bf16[256,512]{1,0:T(8,128)(2,1)} %refs_2_.2, ...), custom_call_target="tpu_custom_call" | custom-call | tf_op jit(solution)/shard_map/pallas_call | solution.py:463
  67.8 1.3 fusion.23
  69.1 2.4 %fusion.30 = (f32[1024]{0:T(1024)S(1)}, f32[1024]{0:T(1024)S(1)}, f32[1024,128]{1,0:T(8,128)S(1)}) fusion(f32[1024,128]{1,0:T(8,128)S(1)} %fusion.23, f32[128]{0:T(128)S(1)} %get-tuple-element.25, f32[128]{0:T(128)S(1)} %get-tuple-element.26, f32[128]{0:T(128)S(1)} %get-tuple-element.27, f32[128]{0:T(128)S(1)} %get-tuple-element.28, ...), kind=kLoop, calls=%fused_computation.108 | loop fusion | flops 8386560 | bytes 1072640 | tf_op jit(solution)/shard_map/reduce_sum | solution.py:797
  71.9 0.7 copy-done
  72.9 0.6 dynamic-slice_reduce_fusion
  74.9 0.5 fusion
  75.4 0.7 fusion.32
  76.1 0.3 copy-done.8
  76.4 0.4 multiply_reduce_fusion.1
  76.8 0.6 select_maximum_fusion.refs_0_
  77.4 8.5 %shard_map.146 = f32[8,1024]{1,0:T(8,128)} custom-call(f32[8,1024]{1,0:T(8,128)} %select_maximum_fusion.refs_0_), custom_call_target="tpu_custom_call" | custom-call | tf_op jit(solution)/shard_map/pallas_call | solution.py:522
  86.0 0.8 slice_multiply_fusion.1
  86.9 0.7 copy-done.11
  87.6 1.0 multiply_convert_fusion.refs_1_
  88.7 0.7 add_rsqrt_fusion.1
  89.4 0.7 copy-done.7
  90.1 0.8 multiply_convert_fusion.2.refs_0_
  90.9 59.1 %shard_map.147 = bf16[128,512]{1,0:T(8,128)(2,1)} custom-call(bf16[256,256]{1,0:T(8,128)(2,1)} %multiply_convert_fusion.2.refs_0_, bf16[1024,128]{1,0:T(8,128)(2,1)} %multiply_convert_fusion.refs_1_, bf16[512,256]{1,0:T(8,128)(2,1)} %refs_2_.3, bf16[256,256]{1,0:T(8,128)(2,1)} %refs_3_.3), custom_call_target="tpu_custom_call" | custom-call | tf_op jit(solution)/shard_map/pallas_call | solution.py:703
  150.0 1.6 %copy.28 = bf16[128,512]{1,0:T(8,128)(2,1)} copy(bf16[128,512]{1,0:T(8,128)(2,1)} %shard_map.147) | data formatting | bytes 262144
  (47 shorter events, 2.1 us)
Async XLA Ops:
  0.0 0.7 copy-start.4
  0.8 0.7 copy-start.3
  0.8 0.7 copy-start.2
  1.8 0.9 copy-start.5
  1.8 0.9 copy-start.6
  69.1 2.5 %copy-start.1 = (f32[8,8,128]{2,1,0:T(8,128)S(1)}, f32[8,8,128]{2,1,0:T(8,128)}, u32[]{:S(2)}) copy-start(f32[8,8,128]{2,1,0:T(8,128)} %get-tuple-element.14) | copy-start | bytes 98308
  71.6 1.0 copy-start
  72.9 2.5 %copy-start.9 = (bf16[1024,256]{1,0:T(8,128)(2,1)S(1)}, bf16[1024,256]{1,0:T(8,128)(2,1)}, u32[]{:S(2)}) copy-start(bf16[1024,256]{1,0:T(8,128)(2,1)} %get-tuple-element.12) | copy-start | bytes 1572868
  73.5 1.8 %copy-start.10 = (bf16[256,256]{1,0:T(8,128)(2,1)S(1)}, bf16[256,256]{1,0:T(8,128)(2,1)}, u32[]{:S(2)}) copy-start(bf16[256,256]{1,0:T(8,128)(2,1)} %get-tuple-element.11) | copy-start | bytes 393220
  75.4 1.0 copy-start.8
  86.9 0.7 copy-start.11
  89.4 0.7 copy-start.7

commit v5 on v4

--- a/solution.py
+++ b/solution.py
@@ -380,7 +380,7 @@
 
     order = line_order(z, layers)
     for index, (source, there, onward, further) in enumerate(order):
-        if index == 2:
+        if index == layers:
             send_weights()
         i = source * 2 + x
         arrived(block(i, tp), token_sem.at[i, tp], there)

time: 153 us -> 141 us (0.922)
  Pallas kernels: 132 us -> 120 us
    pallas_call x1, Pallas kernels: 64.4 us -> 53.9 us  [project(): pl.pallas_call(lambda *refs: project_kernel(count, columns, *refs), out_s...]
    pallas_call x1, Pallas kernels: 59.1 us -> 57.3 us  [mix(): pl.pallas_call(lambda *refs: mix_kernel(count, columns, *refs), out_shape...]
where the time goes in v5:
time: 141 us; the launch traced here: 139 us
  Pallas kernels  120 us (85%)
  other arithmetic  9.78 us (7%)
  local copies, waits for them, and re-layouts  8.42 us (6%)
    pallas_call x1, Pallas kernels, mix(): pl.pallas_call(lambda *refs: mix_kernel(count, columns, *refs), out_shape...  57.3 us
    pallas_call x1, Pallas kernels, project(): pl.pallas_call(lambda *refs: project_kernel(count, columns, *refs), out_s...  53.9 us
    pallas_call x1, Pallas kernels, sum_over_group(): pl.pallas_call(lambda *refs: sums_kernel(count, columns, *refs), out_shap...  8.49 us
    unnamed x25, local copies, waits for them, and re-layouts  5.45 us

profile of v5, /device:TPU:0, one launch (start us, length us, event | category | flops | bytes accessed | tf_op | source)
XLA Modules:
  0.0 139.2 jit_solution(12678173731653911965)
XLA Ops:
  0.0 0.7 copy-done.4
  0.8 0.7 copy-done.3
  1.5 0.3 copy.23
  1.8 0.9 pad.17.refs_6_
  2.8 0.6 pad.18.refs_7_
  3.4 53.9 %shard_map.145 = (f32[1024,256]{1,0:T(8,128)}, f32[1024,128]{1,0:T(8,128)}, bf16[256,256]{1,0:T(8,128)(2,1)}, bf16[1024,256]{1,0:T(8,128)(2,1)}, bf16[1024,256]{1,0:T(8,128)(2,1)}, /*index=5*/f32[8,8,128]{2,1,0:T(8,128)}) custom-call(bf16[128,512]{1,0:T(8,128)(2,1)} %refs_0_.1, bf16[256,512]{1,0:T(8,128)(2,1)} %refs_1_.1, bf16[256,512]{1,0:T(8,128)(2,1)} %refs_2_.2, ...), custom_call_target="tpu_custom_call" | custom-call | tf_op jit(solution)/shard_map/pallas_call | solution.py:463
  57.3 1.3 fusion.23
  58.6 2.4 %fusion.30 = (f32[1024]{0:T(1024)S(1)}, f32[1024]{0:T(1024)S(1)}, f32[1024,128]{1,0:T(8,128)S(1)}) fusion(f32[1024,128]{1,0:T(8,128)S(1)} %fusion.23, f32[128]{0:T(128)S(1)} %get-tuple-element.25, f32[128]{0:T(128)S(1)} %get-tuple-element.26, f32[128]{0:T(128)S(1)} %get-tuple-element.27, f32[128]{0:T(128)S(1)} %get-tuple-element.28, ...), kind=kLoop, calls=%fused_computation.108 | loop fusion | flops 8386560 | bytes 1072640 | tf_op jit(solution)/shard_map/reduce_sum | solution.py:797
  61.4 0.7 copy-done
  62.4 0.6 dynamic-slice_reduce_fusion
  64.4 0.5 fusion
  64.9 0.7 fusion.32
  65.6 0.3 copy-done.8
  65.9 0.4 multiply_reduce_fusion.1
  66.3 0.6 select_maximum_fusion.refs_0_
  66.9 8.5 %shard_map.146 = f32[8,1024]{1,0:T(8,128)} custom-call(f32[8,1024]{1,0:T(8,128)} %select_maximum_fusion.refs_0_), custom_call_target="tpu_custom_call" | custom-call | tf_op jit(solution)/shard_map/pallas_call | solution.py:522
  75.4 0.8 slice_multiply_fusion.1
  76.3 0.7 copy-done.11
  77.1 1.0 multiply_convert_fusion.refs_1_
  78.1 0.7 add_rsqrt_fusion.1
  78.8 0.7 copy-done.7
  79.6 0.8 multiply_convert_fusion.2.refs_0_
  80.3 57.3 %shard_map.147 = bf16[128,512]{1,0:T(8,128)(2,1)} custom-call(bf16[256,256]{1,0:T(8,128)(2,1)} %multiply_convert_fusion.2.refs_0_, bf16[1024,128]{1,0:T(8,128)(2,1)} %multiply_convert_fusion.refs_1_, bf16[512,256]{1,0:T(8,128)(2,1)} %refs_2_.3, bf16[256,256]{1,0:T(8,128)(2,1)} %refs_3_.3), custom_call_target="tpu_custom_call" | custom-call | tf_op jit(solution)/shard_map/pallas_call | solution.py:703
  137.6 1.6 %copy.28 = bf16[128,512]{1,0:T(8,128)(2,1)} copy(bf16[128,512]{1,0:T(8,128)(2,1)} %shard_map.147) | data formatting | bytes 262144
  (47 shorter events, 2.1 us)
Async XLA Ops:
  0.0 0.7 copy-start.4
  0.8 0.7 copy-start.3
  0.8 0.7 copy-start.2
  1.8 0.9 copy-start.5
  1.8 0.9 copy-start.6
  58.6 2.5 %copy-start.1 = (f32[8,8,128]{2,1,0:T(8,128)S(1)}, f32[8,8,128]{2,1,0:T(8,128)}, u32[]{:S(2)}) copy-start(f32[8,8,128]{2,1,0:T(8,128)} %get-tuple-element.14) | copy-start | bytes 98308
  61.1 1.0 copy-start
  62.4 2.5 %copy-start.9 = (bf16[1024,256]{1,0:T(8,128)(2,1)S(1)}, bf16[1024,256]{1,0:T(8,128)(2,1)}, u32[]{:S(2)}) copy-start(bf16[1024,256]{1,0:T(8,128)(2,1)} %get-tuple-element.12) | copy-start | bytes 1572868
  63.0 1.8 %copy-start.10 = (bf16[256,256]{1,0:T(8,128)(2,1)S(1)}, bf16[256,256]{1,0:T(8,128)(2,1)}, u32[]{:S(2)}) copy-start(bf16[256,256]{1,0:T(8,128)(2,1)} %get-tuple-element.11) | copy-start | bytes 393220
  64.9 1.0 copy-start.8
  76.3 0.7 copy-start.11
  78.8 0.7 copy-start.7
